TPU v7x, 256 devices: a 4x2x16 block of a 4x16x16 slice. The times are simulated.
256 devices in a mesh: grp: 2 (over y), sp: 16 (over z), dp: 8 (over x, core).
Axes of the slice: x: 4, y: 2, z: 16, core: 2. Of those that a mesh axis runs over, the one named last changes fastest.
The devices are a block of a 4x16x16 slice.
Arguments:
- activations: bfloat16 [16, 8192, 2048], P(('grp', 'dp'), 'sp'), parts along dimension 0, may hold values from -6 to 6
- value_weight: bfloat16 [2048, 1024], P('sp', 'dp'), may hold values from -0.125 to 0.125
- gate_weight: bfloat16 [2048, 1024], P('sp', 'dp'), may hold values from -0.125 to 0.125
- conv_taps: float32 [31, 1024], replicated, may hold values from -4 to 4
- conv_bias: float32 [1024], replicated, may hold values from -3 to 3
- norm_gain: float32 [1024], replicated, may hold values from 0.1 to 1.9
- norm_bias: float32 [1024], replicated, may hold values from -3 to 3
- out_weight: bfloat16 [1024, 2048], P('sp', 'dp'), may hold values from -0.1875 to 0.1875
Outputs:
- mixed_out: bfloat16 [16, 8192, 2048], P(('grp', 'dp'), 'sp'), parts along dimension 0
There are 2 independent parts, one for each index of `grp`. A program takes and returns all parts, laid end to end along the dimension named above; an argument that names none is the same for every part. Nothing has to cross between parts.
All inputs are finite; a program needn't handle non-finite values.
Results may differ from a plain program's by a relative error of at most 0.013.
Values may be sent and summed in bfloat16 or wider, within the bound.
No kernel may reach another device: no remote copies, remote signals or barrier semaphores. Data moves between devices by JAX's collectives and lax.ppermute only.
A program may use at most 64 MiB of HBM per device.

v0:
```python
import functools

import jax
import jax.numpy as jnp
from jax import lax
from jax.experimental import pallas as pl
from jax.experimental.pallas import tpu as pltpu
from jax.sharding import PartitionSpec as P


epsilon = 1e-05
SCALE = 2.0**18
HALO = 32
ROWS = 64


def whole(space=pltpu.VMEM):
    return pl.BlockSpec(memory_space=space)


def convolve(gated, taps, bias, store, tok_rows):
    kernel_len = taps.shape[0]
    lead = HALO - kernel_len + 1
    for start in range(0, tok_rows, ROWS):
        n_tiles = ROWS // 8
        totals = [bias] * n_tiles
        for shift in range(8):
            near = [(q, 8 * q + shift - lead) for q in range((HALO + 8) // 8)]
            near = [(q, j) for q, j in near if 0 <= j < kernel_len]
            weights = [(q, taps[j]) for q, j in near]
            for m in range(n_tiles + near[-1][0]):
                users = [(m - q, w) for q, w in weights if 0 <= m - q < n_tiles]
                if not users:
                    continue
                row = gated[pl.ds(start + 8 * m + shift, 8), :]
                for tile, w in users:
                    totals[tile] = totals[tile] + w * row
        for tile, total in enumerate(totals):
            store(start + 8 * tile, total)


def conv_kernel(counts, first, n_done, index_ref, taps_ref, bias_ref, *refs):
    n_pieces, n_blocks = sum(counts), len(counts)
    norm = n_done > 0
    if norm:
        (gain_ref, shift_ref), refs = refs[:2], refs[2:]
    rows_hbm, pieces, refs = refs[0], refs[1 : 1 + n_pieces], refs[1 + n_pieces :]
    done, refs = refs[:n_done], refs[n_done:]
    n_outs = 1 if norm else n_blocks
    outs, refs = refs[:n_outs], refs[n_outs:]
    rows, held, gated, taps_held, sems, conv = refs
    tok_rows, width = rows.shape[0] - HALO, gated.shape[-1]
    kernel_len = taps_ref.shape[0]

    copies = [pltpu.make_async_copy(rows_hbm, rows, sems.at[0])]
    at = 0
    for k, count in enumerate(counts):
        depth = 0
        for _ in range(count):
            size = pieces[at].shape[0]
            copies.append(pltpu.make_async_copy(pieces[at], held.at[k, pl.ds(depth, size), :], sems.at[1 + at]))
            depth += size
            at += 1
    for k in range(n_done):
        copies.append(pltpu.make_async_copy(done[k], conv.at[k], sems.at[1 + n_pieces + k]))
    for copy in copies:
        copy.start()

    def lane_of(k):
        return pl.multiple_of(index_ref[first + k] * width, width)

    def project(k):
        at = 1 + sum(counts[:k])
        for copy in copies[at : at + counts[k]]:
            copy.wait()
        return jnp.dot(rows[...], held[k], preferred_element_type=jnp.float32)

    def gate(k, both):
        value = both[:, :width].astype(jnp.bfloat16).astype(jnp.float32)
        gates = both[:, width:].astype(jnp.bfloat16).astype(jnp.float32)
        gated[k % 2] = (value * jax.nn.sigmoid(gates)).astype(jnp.bfloat16).astype(jnp.float32)
        for j in range(kernel_len):
            taps_held[k % 2, j] = jnp.broadcast_to(taps_ref[j : j + 1, pl.ds(lane_of(k), width)], (8, width))

    def filter_block(k):
        bias = jnp.broadcast_to(bias_ref[:, pl.ds(lane_of(k), width)], (8, width))

        def store(at, value):
            if norm:
                conv[n_done + k, pl.ds(at, 8), :] = value
            else:
                outs[k][pl.ds(at, 8), :] = value

        convolve(gated.at[k % 2], taps_held.at[k % 2], bias, store, tok_rows)

    copies[0].wait()
    gate(0, project(0))
    for k in range(1, n_blocks):
        both = project(k)
        filter_block(k - 1)
        gate(k, both)
    filter_block(n_blocks - 1)
    for copy in copies[1 + n_pieces :]:
        copy.wait()
    if not norm:
        return

    out = outs[0]
    total = n_done + n_blocks
    lanes = [pl.multiple_of(index_ref[k] * width, width) for k in range(total)]

    def tile(i, carry):
        at = pl.ds(pl.multiple_of(i * 16, 16), 16)
        values = [conv[k, at, :] for k in range(total)]
        mean = jnp.sum(sum(values[1:], values[0]), axis=-1, keepdims=True) / (total * width)
        values = [v - mean for v in values]
        squares = [v * v for v in values]
        spread = jnp.sum(sum(squares[1:], squares[0]), axis=-1, keepdims=True) / (total * width)
        scale = lax.rsqrt(spread + epsilon)
        for v, lane in zip(values, lanes):
            normed = v * scale * gain_ref[:, pl.ds(lane, width)] + shift_ref[:, pl.ds(lane, width)]
            out[at, pl.ds(lane, width)] = jax.nn.silu(normed).astype(jnp.bfloat16)
        return carry

    lax.fori_loop(0, tok_rows // 16, tile, 0, unroll=4)


def conv_blocks(rows, blocks, index, first, taps, bias, done=(), gain=None, shift=None):
    tok_rows = rows.shape[0] - HALO
    width = blocks[0][0].shape[1] // 2
    counts = tuple(len(b) for b in blocks)
    pieces = [p for b in blocks for p in b]
    n_blocks, n_done = len(blocks), len(done)
    norm = n_done > 0
    if norm:
        outs = [jax.ShapeDtypeStruct((tok_rows, width * (n_done + n_blocks)), jnp.bfloat16)]
    else:
        outs = [jax.ShapeDtypeStruct((tok_rows, width), jnp.float32) for _ in blocks]
    flops = 2 * rows.shape[0] * rows.shape[1] * 2 * width * n_blocks
    return pl.pallas_call(
        functools.partial(conv_kernel, counts, first, n_done),
        out_shape=outs,
        in_specs=[whole(pltpu.SMEM)]
        + [whole()] * (4 if norm else 2)
        + [whole(pl.ANY)] * (1 + len(pieces) + n_done),
        out_specs=[whole()] * len(outs),
        scratch_shapes=[
            pltpu.VMEM(rows.shape, rows.dtype),
            pltpu.VMEM((n_blocks, rows.shape[1], 2 * width), rows.dtype),
            pltpu.VMEM((2, rows.shape[0], width), jnp.float32),
            pltpu.VMEM((2, taps.shape[0], 8, width), jnp.float32),
            pltpu.SemaphoreType.DMA((1 + len(pieces) + n_done,)),
            pltpu.VMEM((n_done + n_blocks, tok_rows, width) if norm else (1, 8, width), jnp.float32),
        ],
        cost_estimate=pl.CostEstimate(flops=flops, bytes_accessed=rows.size * 2, transcendentals=0),
        name="conv_norm" if norm else "conv_blocks",
    )(index, taps, bias, *((gain, shift) if norm else ()), rows, *pieces, *done)


def out_kernel(counts, first, index_ref, rows_ref, *refs):
    n_pieces = sum(counts)
    pieces = refs[:n_pieces]
    out, held, sems = refs[-3:]
    begin = 0
    copies = []
    for k, count in enumerate(counts):
        total = None
        at = 0
        for piece in pieces[begin : begin + count]:
            depth, width = piece.shape
            part = jnp.dot(rows_ref[:, at : at + depth], piece[...], preferred_element_type=jnp.float32)
            total = part if total is None else total + part
            at += depth
        begin += count
        held[k] = total.astype(jnp.bfloat16)
        lane = pl.multiple_of(index_ref[first + k] * width, width)
        copies.append(pltpu.make_async_copy(held.at[k], out.at[:, pl.ds(lane, width)], sems.at[k]))
        copies[-1].start()
    for copy in copies:
        copy.wait()


def out_blocks(rows, blocks, index, first, n_blocks, base=None):
    width = blocks[0][0].shape[1]
    counts = tuple(len(b) for b in blocks)
    pieces = [p for b in blocks for p in b]
    more = [] if base is None else [base]
    return pl.pallas_call(
        functools.partial(out_kernel, counts, first),
        out_shape=jax.ShapeDtypeStruct((rows.shape[0], width * n_blocks), jnp.bfloat16),
        in_specs=[whole(pltpu.SMEM)] + [whole()] * (1 + len(pieces)) + [whole(pl.ANY)] * len(more),
        out_specs=whole(pl.ANY),
        scratch_shapes=[
            pltpu.VMEM((len(blocks), rows.shape[0], width), jnp.bfloat16),
            pltpu.SemaphoreType.DMA((len(blocks),)),
        ],
        input_output_aliases={2 + len(pieces): 0} if more else {},
        cost_estimate=pl.CostEstimate(flops=2 * rows.size * width * len(blocks), bytes_accessed=rows.size * 6, transcendentals=0),
        name="out_blocks",
    )(index, rows, *pieces, *more)


def work(activations, value_weight, gate_weight, conv_taps, conv_bias, norm_gain, norm_bias, out_weight):
    tokens = activations[0]
    n_sp, n_dp = lax.axis_size("sp"), lax.axis_size("dp")
    me = lax.axis_index("dp")

    def from_next(a):
        return lax.ppermute(a, "dp", [(i, (i - 2) % n_dp) for i in range(n_dp)])

    def from_last(a):
        return lax.ppermute(a, "dp", [(i, (i + 2) % n_dp) for i in range(n_dp)])

    def from_core(a):
        return lax.ppermute(a, "dp", [(i, i ^ 1) for i in range(n_dp)])

    halo = lax.ppermute(tokens[-HALO:], "sp", [(i, i + 1) for i in range(n_sp - 1)])

    hold = lax.optimization_barrier
    depth = value_weight.shape[0]
    packed = jnp.concatenate([jnp.concatenate([value_weight, gate_weight], axis=1), out_weight], axis=0)
    packed = (packed.astype(jnp.float32) * SCALE).astype(jnp.float16)
    packed, halo = hold((packed, halo))
    packed = lax.all_gather(packed, "sp", axis=0)
    packed = (packed.astype(jnp.float32) * (1.0 / SCALE)).astype(jnp.bfloat16)
    width = packed.shape[-1]
    upper = packed[: n_sp // 2, :depth].reshape(-1, width)
    lower = packed[n_sp // 2 :, :depth].reshape(-1, width)
    o_own = packed[:, depth:].reshape(-1, width)
    o_half = o_own.shape[0] // 2
    bias, gain, shift = conv_bias[None, :], norm_gain[None, :], norm_bias[None, :]
    place = jnp.arange(n_dp, dtype=jnp.int32)
    chip = place // 2
    step = jnp.where(chip == 2, -2, jnp.where(chip == 3, 4, 2 * chip))
    index = ((me + step) % n_dp) ^ (place % 2)

    next_a, last_b = from_next(upper), from_last(lower)
    next_b, last_a = from_next(lower), from_last(upper)
    rows = jnp.concatenate([halo, tokens], axis=0)
    own_swap = [from_core(upper), from_core(lower)]
    conv_a = conv_blocks(rows, [[upper, lower], own_swap], index, 0, conv_taps, bias)
    next_a, last_b, conv_a = hold((next_a, last_b, conv_a))
    far_a, far_b = from_next(next_a), from_last(last_b)
    next_b, last_a, o_send = hold((next_b, last_a, o_own))
    o_next, o_last = from_next(o_send), from_last(o_send)
    o_swap = from_core(o_send)
    swaps = [[from_core(next_a), from_core(next_b)], [from_core(last_a), from_core(last_b)]]
    conv_b = conv_blocks(
        rows, [[next_a, next_b], swaps[0], [last_a, last_b], swaps[1]], index, 2, conv_taps, bias
    )
    far_a, far_b, conv_b = hold((far_a, far_b, conv_b))
    (swished,) = conv_blocks(
        rows, [[far_a, far_b], [from_core(far_a), from_core(far_b)]], index, 6, conv_taps, bias,
        conv_a + conv_b, gain, shift,
    )
    o_next, o_last, swished = hold((o_next, o_last, swished))
    o_far_a, o_far_b = from_next(o_next[:o_half]), from_last(o_last[o_half:])
    o_swaps = from_core(o_next), from_core(o_last)
    result = out_blocks(
        swished, [[o_send], [o_swap], [o_next], [o_swaps[0]], [o_last], [o_swaps[1]]], index, 0, n_dp
    )
    o_far_a, o_far_b, result = hold((o_far_a, o_far_b, result))
    result = out_blocks(
        swished, [[o_far_a, o_far_b], [from_core(o_far_a), from_core(o_far_b)]], index, 6, n_dp, result
    )
    return result[None]


def solution(mesh):
    in_specs = (
        P(("grp", "dp"), "sp", None),
        P("sp", "dp"),
        P("sp", "dp"),
        P(),
        P(),
        P(),
        P(),
        P("sp", "dp"),
    )
    out_specs = P(("grp", "dp"), "sp", None)
    return jax.shard_map(work, mesh=mesh, in_specs=in_specs, out_specs=out_specs, check_vma=False)
```

profile of v0, /device:TPU:33, one launch (start us, length us, event | category | flops | bytes accessed | tf_op | source)
XLA Modules:
  0.0 150.6 jit_solution(7795760867308370384)
XLA Ops:
  0.0 0.9 slice_bitcast_fusion
  0.9 5.3 %collective-permute-start = (bf16[32,2048]{1,0:T(8,128)(2,1)S(1)}, bf16[32,2048]{1,0:T(8,128)(2,1)S(1)}, u32[]{:S(2)}, u32[]{:S(2)}) collective-permute-start(bf16[32,2048]{1,0:T(8,128)(2,1)S(1)} %slice_bitcast_fusion), channel_id=1, source_target_pairs={{0,8},{8,16},{16,24},{24,32},{32,40},{40,48},{48,56},{56,64},{64,7... | collective-permute-start | bytes 393224 | tf_op jit(solution)/shard_map/ppermute | solution.py:217
  6.2 0.8 multiply_convert_fusion.1
  7.0 1.1 collective-permute-done
  8.1 51.5 %all-gather.2 = f16[3072,256]{1,0:T(8,128)(2,1)S(1)} all-gather(f16[192,256]{1,0:T(8,128)(2,1)S(1)} %multiply_convert_fusion.1), channel_id=2, replica_groups=mesh['grp'=2,'sp'=16,'dp'=8] {'sp'}, dimensions={0}, use_global_device_ids=true | all-gather | bytes 1671168 | tf_op jit(solution)/shard_map/all_gather | solution.py:224
  59.6 0.4 multiply_convert_fusion
  60.0 0.1 fusion.3
  60.1 0.0 copy-start.1
  60.1 8.6 %collective-permute-start.7 = (bf16[1024,256]{1,0:T(8,128)(2,1)S(1)}, bf16[1024,256]{1,0:T(8,128)(2,1)S(1)}, u32[]{:S(2)}, u32[]{:S(2)}) collective-permute-start(bf16[1024,256]{1,0:T(8,128)(2,1)S(1)} %bitcast.18), channel_id=1, source_target_pairs={{0,1},{1,0},{2,3},{3,2},{4,5},{5,4},{6,7},{7,6},{8,9},{9,8},{10,11... | collective-permute-start | bytes 1572872 | tf_op jit(solution)/shard_map/ppermute | solution.py:215
  68.7 0.1 collective-permute-start.8
  68.9 2.9 %collective-permute-start.5 = (bf16[1024,256]{1,0:T(8,128)(2,1)S(1)}, bf16[1024,256]{1,0:T(8,128)(2,1)}, u32[]{:S(2)}, u32[]{:S(2)}) collective-permute-start(bf16[1024,256]{1,0:T(8,128)(2,1)S(1)} %bitcast.19), channel_id=1, source_target_pairs={{0,6},{1,7},{2,0},{3,1},{4,2},{5,3},{6,4},{7,5},{8,14},{9,15},{10,... | collective-permute-start | bytes 1572872 | tf_op jit(solution)/shard_map/ppermute | solution.py:209
  71.8 0.0 collective-permute-start.6
  71.8 0.6 fusion.index_ref
  72.3 2.7 %collective-permute-start.1 = (bf16[1024,256]{1,0:T(8,128)(2,1)S(1)}, bf16[1024,256]{1,0:T(8,128)(2,1)}, u32[]{:S(2)}, u32[]{:S(2)}) collective-permute-start(bf16[1024,256]{1,0:T(8,128)(2,1)S(1)} %bitcast.24), channel_id=1, source_target_pairs={{0,6},{1,7},{2,0},{3,1},{4,2},{5,3},{6,4},{7,5},{8,14},{9,15},{10,... | collective-permute-start | bytes 1572872 | tf_op jit(solution)/shard_map/ppermute | solution.py:209
  75.0 3.4 %pad_maximum_fusion.refs_0_.refs_2_ = bf16[544,2048]{1,0:T(8,128)(2,1)} fusion(bf16[512,2048]{1,0:T(8,128)(2,1)} %bitcast.13, bf16[32,2048]{1,0:T(8,128)(2,1)S(1)} %collective-permute-done), kind=kLoop, calls=%fused_computation.1 | loop fusion | flops 4456448 | bytes 4456448 | tf_op jit(solution)/shard_map/concatenate | solution.py:239
  78.5 0.0 collective-permute-done.8.refs_4_
  78.5 7.2 %conv_blocks.2 = (f32[512,128]{1,0:T(8,128)}, f32[512,128]{1,0:T(8,128)}) custom-call(s32[8]{0:T(128)} %fusion.index_ref, f32[31,1024]{1,0:T(8,128)} %taps_ref.5, f32[1,1024]{1,0:T(1,128)} %bitcast.26, bf16[544,2048]{1,0:T(8,128)(2,1)} %pad_maximum_fusion.refs_0_.refs_2_, bf16[1024,256]{1,0:T(8,128)(2,1)} %bitcast.21, bf16[1024,256]{1,0:T(8,128)(2,1)} %bitcast.25, ...), custom_call_target="tpu_custom_call" | custom-call | flops 1140850688 | bytes 2228224 | tf_op jit(solution)/shard_map/conv_blocks/pallas_call | solution.py:140
  85.7 0.2 collective-permute-done.6.refs_6_
  85.9 2.6 %collective-permute-start.11 = (bf16[1024,256]{1,0:T(8,128)(2,1)}, bf16[1024,256]{1,0:T(8,128)(2,1)}, u32[]{:S(2)}, u32[]{:S(2)}) collective-permute-start(bf16[1024,256]{1,0:T(8,128)(2,1)} %collective-permute-done.5.refs_1_), channel_id=1, source_target_pairs={{0,1},{1,0},{2,3},{3,2},{4,5},{5,4},{6,7},{7,6},{8,9},{9,8},{10,11... | collective-permute-start | bytes 1572872 | tf_op jit(solution)/shard_map/ppermute | solution.py:215
  88.6 0.1 collective-permute-start.14
  88.7 5.2 %collective-permute-done.1.refs_2_ = bf16[1024,256]{1,0:T(8,128)(2,1)} collective-permute-done((bf16[1024,256]{1,0:T(8,128)(2,1)S(1)}, bf16[1024,256]{1,0:T(8,128)(2,1)}, u32[]{:S(2)}, u32[]{:S(2)}) %collective-permute-start.1) | collective-permute-done | bytes 524320 | tf_op jit(solution)/shard_map/ppermute | solution.py:209
  93.9 3.2 %collective-permute-done.2.refs_5_ = bf16[1024,256]{1,0:T(8,128)(2,1)} collective-permute-done((bf16[1024,256]{1,0:T(8,128)(2,1)S(1)}, bf16[1024,256]{1,0:T(8,128)(2,1)}, u32[]{:S(2)}, u32[]{:S(2)}) %collective-permute-start.2) | collective-permute-done | bytes 524320 | tf_op jit(solution)/shard_map/ppermute | solution.py:212
  97.1 1.5 collective-permute-start.12
  98.6 0.0 collective-permute-start.13
  98.6 0.0 collective-permute-start.10
  98.6 0.0 collective-permute-done.11.refs_3_
  98.7 2.7 %collective-permute-start.9 = (bf16[1024,256]{1,0:T(8,128)(2,1)}, bf16[1024,256]{1,0:T(8,128)(2,1)S(1)}, u32[]{:S(2)}, u32[]{:S(2)}) collective-permute-start(bf16[1024,256]{1,0:T(8,128)(2,1)} %collective-permute-done.5.refs_1_), channel_id=1, source_target_pairs={{0,6},{1,7},{2,0},{3,1},{4,2},{5,3},{6,4},{7,5},{8,14},{9,15},{10,... | collective-permute-start | bytes 1572872 | tf_op jit(solution)/shard_map/ppermute | solution.py:209
  101.3 0.0 collective-permute-done.14.refs_8_
  101.3 0.0 collective-permute-done.12.refs_4_
  101.3 0.0 copy-start.17
  101.4 0.8 copy-done.16
  102.1 0.2 copy-done.17
  102.3 0.8 copy-done.18
  103.1 11.0 %conv_blocks.3 = (f32[512,128]{1,0:T(8,128)}, f32[512,128]{1,0:T(8,128)}, f32[512,128]{1,0:T(8,128)}, f32[512,128]{1,0:T(8,128)}) custom-call(s32[8]{0:T(128)} %fusion.index_ref, f32[31,1024]{1,0:T(8,128)} %taps_ref.5, f32[1,1024]{1,0:T(1,128)} %bitcast.27, bf16[544,2048]{1,0:T(8,128)(2,1)} %pad_maximum_fusion.refs_0_.refs_2_, ...), custom_call_target="tpu_custom_call" | custom-call | flops 2281701376 | bytes 2228224 | tf_op jit(solution)/shard_map/conv_blocks/pallas_call | solution.py:140
  114.1 0.0 collective-permute-done.9.refs_3_
  114.1 0.0 copy-start.9
  114.1 1.2 collective-permute-start.15
  115.3 0.1 collective-permute-start.16
  115.5 1.6 %collective-permute-start.3 = (bf16[1024,256]{1,0:T(8,128)(2,1)S(1)}, bf16[1024,256]{1,0:T(8,128)(2,1)S(1)}, u32[]{:S(2)}, u32[]{:S(2)}) collective-permute-start(bf16[1024,256]{1,0:T(8,128)(2,1)S(1)} %bitcast.14), channel_id=1, source_target_pairs={{0,6},{1,7},{2,0},{3,1},{4,2},{5,3},{6,4},{7,5},{8,14},{9,15},{10,... | collective-permute-start | bytes 1572872 | tf_op jit(solution)/shard_map/ppermute | solution.py:209
  117.1 0.0 collective-permute-start.4
  117.1 0.8 collective-permute-start.19
  117.9 0.0 collective-permute-done.15.refs_5_
  117.9 0.8 copy-done.11
  118.7 0.8 copy-done.12
  119.5 9.5 %conv_norm.1.rows_ref = bf16[512,1024]{1,0:T(8,128)(2,1)} custom-call(s32[8]{0:T(128)} %fusion.index_ref, f32[31,1024]{1,0:T(8,128)} %taps_ref.5, f32[1,1024]{1,0:T(1,128)} %bitcast.28, f32[1,1024]{1,0:T(1,128)} %bitcast.29, f32[1,1024]{1,0:T(1,128)} %bitcast.30, bf16[544,2048]{1,0:T(8,128)(2,1)} %pad_maximum_fusion.refs_0_.refs_2_, ...), custom_call_target="tpu_custom_call" | custom-call | flops 1140850688 | bytes 2228224 | tf_op jit(solution)/shard_map/conv_norm/pallas_call | solution.py:140
  129.0 2.0 %collective-permute-done.4.refs_4_ = bf16[1024,256]{1,0:T(8,128)(2,1)S(1)} collective-permute-done((bf16[1024,256]{1,0:T(8,128)(2,1)S(1)}, bf16[1024,256]{1,0:T(8,128)(2,1)S(1)}, u32[]{:S(2)}, u32[]{:S(2)}) %collective-permute-start.4) | collective-permute-done | bytes 524320 | tf_op jit(solution)/shard_map/ppermute | solution.py:212
  131.0 1.6 %collective-permute-start.20 = (bf16[1024,256]{1,0:T(8,128)(2,1)S(1)}, bf16[1024,256]{1,0:T(8,128)(2,1)S(1)}, u32[]{:S(2)}, u32[]{:S(2)}) collective-permute-start(bf16[1024,256]{1,0:T(8,128)(2,1)S(1)} %collective-permute-done.3.refs_2_), channel_id=1, source_target_pairs={{0,1},{1,0},{2,3},{3,2},{4,5},{5,4},{6,7},{7,6},{8,9},{9,8},{10,11... | collective-permute-start | bytes 1572872 | tf_op jit(solution)/shard_map/ppermute | solution.py:215
  132.6 0.0 collective-permute-start.21
  132.7 0.7 slice.26
  133.4 0.7 slice.27
  134.1 0.5 collective-permute-start.17
  134.6 1.0 collective-permute-start.18
  135.6 0.8 copy-done.5
  136.4 0.2 copy-done.6
  136.5 0.8 copy-done.7
  137.3 4.8 %out_blocks.2.refs_4_ = bf16[512,2048]{1,0:T(8,128)(2,1)} custom-call(s32[8]{0:T(128)} %fusion.index_ref, bf16[512,1024]{1,0:T(8,128)(2,1)} %conv_norm.1.rows_ref, bf16[1024,256]{1,0:T(8,128)(2,1)} %bitcast.17, bf16[1024,256]{1,0:T(8,128)(2,1)} %copy-done.5, bf16[1024,256]{1,0:T(8,128)(2,1)} %copy-done.3, bf16[1024,256]{1,0:T(8,128)(2,1)} %copy-done.6, ...), custom_call_target="tpu_custom_call" | custom-call | flops 1610612736 | bytes 3145728 | tf_op jit(solution)/shard_map/out_blocks/pallas_call | solution.py:188
  142.2 1.3 collective-permute-done.18.refs_1_
  143.5 1.3 collective-permute-start.22
  144.8 0.0 collective-permute-start.23
  144.8 1.2 collective-permute-done.22.refs_2_
  146.0 0.6 collective-permute-done.23.refs_3_
  146.6 0.1 copy-done.14
  146.7 0.7 copy-done.15
  147.4 3.0 %out_blocks.3 = bf16[512,2048]{1,0:T(8,128)(2,1)} custom-call(s32[8]{0:T(128)} %fusion.index_ref, bf16[512,1024]{1,0:T(8,128)(2,1)} %conv_norm.1.rows_ref, bf16[512,256]{1,0:T(8,128)(2,1)} %copy-done.13, bf16[512,256]{1,0:T(8,128)(2,1)} %collective-permute-done.18.refs_1_, bf16[512,256]{1,0:T(8,128)(2,1)} %copy-done.14, ...), custom_call_target="tpu_custom_call", output_to_operand_aliasing={{}: (6, {})} | custom-call | flops 536870912 | bytes 3145728 | tf_op jit(solution)/shard_map/out_blocks/pallas_call | solution.py:188
  (37 shorter events, 0.1 us)
Async XLA Ops:
  0.9 7.2 %collective-permute-start = (bf16[32,2048]{1,0:T(8,128)(2,1)S(1)}, bf16[32,2048]{1,0:T(8,128)(2,1)S(1)}, u32[]{:S(2)}, u32[]{:S(2)}) collective-permute-start(bf16[32,2048]{1,0:T(8,128)(2,1)S(1)} %slice_bitcast_fusion), channel_id=1, source_target_pairs={{0,8},{8,16},{16,24},{24,32},{32,40},{40,48},{48,56},{56,64},{64,7... | collective-permute-start | bytes 393224 | tf_op jit(solution)/shard_map/ppermute | solution.py:217
  60.1 18.4 %copy-start.1 = (bf16[8,128,256]{2,1,0:T(8,128)(2,1)}, bf16[8,128,256]{2,1,0:T(8,128)(2,1)S(1)}, u32[]{:S(2)}) copy-start(bf16[8,128,256]{2,1,0:T(8,128)(2,1)S(1)} %get-tuple-element.59) | copy-start | bytes 1572868
  60.1 18.4 %copy-start.2 = (bf16[8,128,256]{2,1,0:T(8,128)(2,1)}, bf16[8,128,256]{2,1,0:T(8,128)(2,1)S(1)}, u32[]{:S(2)}) copy-start(bf16[8,128,256]{2,1,0:T(8,128)(2,1)S(1)} %get-tuple-element.60) | copy-start | bytes 1572868
  60.1 14.9 %collective-permute-start.7 = (bf16[1024,256]{1,0:T(8,128)(2,1)S(1)}, bf16[1024,256]{1,0:T(8,128)(2,1)S(1)}, u32[]{:S(2)}, u32[]{:S(2)}) collective-permute-start(bf16[1024,256]{1,0:T(8,128)(2,1)S(1)} %bitcast.18), channel_id=1, source_target_pairs={{0,1},{1,0},{2,3},{3,2},{4,5},{5,4},{6,7},{7,6},{8,9},{9,8},{10,11... | collective-permute-start | bytes 1572872 | tf_op jit(solution)/shard_map/ppermute | solution.py:215
  68.7 9.7 %collective-permute-start.8 = (bf16[1024,256]{1,0:T(8,128)(2,1)S(1)}, bf16[1024,256]{1,0:T(8,128)(2,1)}, u32[]{:S(2)}, u32[]{:S(2)}) collective-permute-start(bf16[1024,256]{1,0:T(8,128)(2,1)S(1)} %bitcast.22), channel_id=1, source_target_pairs={{0,1},{1,0},{2,3},{3,2},{4,5},{5,4},{6,7},{7,6},{8,9},{9,8},{10,11... | collective-permute-start | bytes 1572872 | tf_op jit(solution)/shard_map/ppermute | solution.py:215
  68.9 16.9 %collective-permute-start.5 = (bf16[1024,256]{1,0:T(8,128)(2,1)S(1)}, bf16[1024,256]{1,0:T(8,128)(2,1)}, u32[]{:S(2)}, u32[]{:S(2)}) collective-permute-start(bf16[1024,256]{1,0:T(8,128)(2,1)S(1)} %bitcast.19), channel_id=1, source_target_pairs={{0,6},{1,7},{2,0},{3,1},{4,2},{5,3},{6,4},{7,5},{8,14},{9,15},{10,... | collective-permute-start | bytes 1572872 | tf_op jit(solution)/shard_map/ppermute | solution.py:209
  71.8 14.2 %collective-permute-start.6 = (bf16[1024,256]{1,0:T(8,128)(2,1)S(1)}, bf16[1024,256]{1,0:T(8,128)(2,1)}, u32[]{:S(2)}, u32[]{:S(2)}) collective-permute-start(bf16[1024,256]{1,0:T(8,128)(2,1)S(1)} %bitcast.23), channel_id=1, source_target_pairs={{0,2},{1,3},{2,4},{3,5},{4,6},{5,7},{6,0},{7,1},{8,10},{9,11},{10,... | collective-permute-start | bytes 1572872 | tf_op jit(solution)/shard_map/ppermute | solution.py:212
  72.3 21.6 %collective-permute-start.1 = (bf16[1024,256]{1,0:T(8,128)(2,1)S(1)}, bf16[1024,256]{1,0:T(8,128)(2,1)}, u32[]{:S(2)}, u32[]{:S(2)}) collective-permute-start(bf16[1024,256]{1,0:T(8,128)(2,1)S(1)} %bitcast.24), channel_id=1, source_target_pairs={{0,6},{1,7},{2,0},{3,1},{4,2},{5,3},{6,4},{7,5},{8,14},{9,15},{10,... | collective-permute-start | bytes 1572872 | tf_op jit(solution)/shard_map/ppermute | solution.py:209
  75.0 3.4 %copy-start.10 = (bf16[1024,256]{1,0:T(8,128)(2,1)}, bf16[1024,256]{1,0:T(8,128)(2,1)S(1)}, u32[]{:S(2)}) copy-start(bf16[1024,256]{1,0:T(8,128)(2,1)S(1)} %collective-permute-done.7.refs_3_) | copy-start | bytes 1572868
  75.0 22.1 %collective-permute-start.2 = (bf16[1024,256]{1,0:T(8,128)(2,1)S(1)}, bf16[1024,256]{1,0:T(8,128)(2,1)}, u32[]{:S(2)}, u32[]{:S(2)}) collective-permute-start(bf16[1024,256]{1,0:T(8,128)(2,1)S(1)} %bitcast.20), channel_id=1, source_target_pairs={{0,2},{1,3},{2,4},{3,5},{4,6},{5,7},{6,0},{7,1},{8,10},{9,11},{10,... | collective-permute-start | bytes 1572872 | tf_op jit(solution)/shard_map/ppermute | solution.py:212
  85.9 12.7 %collective-permute-start.11 = (bf16[1024,256]{1,0:T(8,128)(2,1)}, bf16[1024,256]{1,0:T(8,128)(2,1)}, u32[]{:S(2)}, u32[]{:S(2)}) collective-permute-start(bf16[1024,256]{1,0:T(8,128)(2,1)} %collective-permute-done.5.refs_1_), channel_id=1, source_target_pairs={{0,1},{1,0},{2,3},{3,2},{4,5},{5,4},{6,7},{7,6},{8,9},{9,8},{10,11... | collective-permute-start | bytes 1572872 | tf_op jit(solution)/shard_map/ppermute | solution.py:215
  88.6 28.5 %copy-start = (bf16[16,64,256]{2,1,0:T(8,128)(2,1)}, bf16[16,64,256]{2,1,0:T(8,128)(2,1)S(1)}, u32[]{:S(2)}) copy-start(bf16[16,64,256]{2,1,0:T(8,128)(2,1)S(1)} %slice.30) | copy-start | bytes 1572868
  88.6 12.8 %collective-permute-start.14 = (bf16[1024,256]{1,0:T(8,128)(2,1)}, bf16[1024,256]{1,0:T(8,128)(2,1)S(1)}, u32[]{:S(2)}, u32[]{:S(2)}) collective-permute-start(bf16[1024,256]{1,0:T(8,128)(2,1)} %collective-permute-done.6.refs_6_), channel_id=1, source_target_pairs={{0,1},{1,0},{2,3},{3,2},{4,5},{5,4},{6,7},{7,6},{8,9},{9,8},{10,11... | collective-permute-start | bytes 1572872 | tf_op jit(solution)/shard_map/ppermute | solution.py:215
  97.1 4.2 %collective-permute-start.12 = (bf16[1024,256]{1,0:T(8,128)(2,1)}, bf16[1024,256]{1,0:T(8,128)(2,1)S(1)}, u32[]{:S(2)}, u32[]{:S(2)}) collective-permute-start(bf16[1024,256]{1,0:T(8,128)(2,1)} %collective-permute-done.1.refs_2_), channel_id=1, source_target_pairs={{0,1},{1,0},{2,3},{3,2},{4,5},{5,4},{6,7},{7,6},{8,9},{9,8},{10,11... | collective-permute-start | bytes 1572872 | tf_op jit(solution)/shard_map/ppermute | solution.py:215
  98.6 2.7 %collective-permute-start.13 = (bf16[1024,256]{1,0:T(8,128)(2,1)}, bf16[1024,256]{1,0:T(8,128)(2,1)S(1)}, u32[]{:S(2)}, u32[]{:S(2)}) collective-permute-start(bf16[1024,256]{1,0:T(8,128)(2,1)} %collective-permute-done.2.refs_5_), channel_id=1, source_target_pairs={{0,1},{1,0},{2,3},{3,2},{4,5},{5,4},{6,7},{7,6},{8,9},{9,8},{10,11... | collective-permute-start | bytes 1572872 | tf_op jit(solution)/shard_map/ppermute | solution.py:215
  98.6 15.4 %collective-permute-start.10 = (bf16[1024,256]{1,0:T(8,128)(2,1)}, bf16[1024,256]{1,0:T(8,128)(2,1)S(1)}, u32[]{:S(2)}, u32[]{:S(2)}) collective-permute-start(bf16[1024,256]{1,0:T(8,128)(2,1)} %collective-permute-done.6.refs_6_), channel_id=1, source_target_pairs={{0,2},{1,3},{2,4},{3,5},{4,6},{5,7},{6,0},{7,1},{8,10},{9,11},{10,... | collective-permute-start | bytes 1572872 | tf_op jit(solution)/shard_map/ppermute | solution.py:212
  98.7 15.5 %collective-permute-start.9 = (bf16[1024,256]{1,0:T(8,128)(2,1)}, bf16[1024,256]{1,0:T(8,128)(2,1)S(1)}, u32[]{:S(2)}, u32[]{:S(2)}) collective-permute-start(bf16[1024,256]{1,0:T(8,128)(2,1)} %collective-permute-done.5.refs_1_), channel_id=1, source_target_pairs={{0,6},{1,7},{2,0},{3,1},{4,2},{5,3},{6,4},{7,5},{8,14},{9,15},{10,... | collective-permute-start | bytes 1572872 | tf_op jit(solution)/shard_map/ppermute | solution.py:209
  101.3 0.8 copy-start.16
  101.3 1.0 copy-start.17
  102.3 0.8 copy-start.18
  114.1 5.4 %copy-start.8 = (bf16[1024,256]{1,0:T(8,128)(2,1)}, bf16[1024,256]{1,0:T(8,128)(2,1)S(1)}, u32[]{:S(2)}) copy-start(bf16[1024,256]{1,0:T(8,128)(2,1)S(1)} %collective-permute-done.10.refs_4_) | copy-start | bytes 1572868
  114.1 5.4 %copy-start.9 = (bf16[1024,256]{1,0:T(8,128)(2,1)}, bf16[1024,256]{1,0:T(8,128)(2,1)S(1)}, u32[]{:S(2)}) copy-start(bf16[1024,256]{1,0:T(8,128)(2,1)S(1)} %collective-permute-done.9.refs_3_) | copy-start | bytes 1572868
  114.1 3.8 %collective-permute-start.15 = (bf16[1024,256]{1,0:T(8,128)(2,1)S(1)}, bf16[1024,256]{1,0:T(8,128)(2,1)S(1)}, u32[]{:S(2)}, u32[]{:S(2)}) collective-permute-start(bf16[1024,256]{1,0:T(8,128)(2,1)S(1)} %collective-permute-done.9.refs_3_), channel_id=1, source_target_pairs={{0,1},{1,0},{2,3},{3,2},{4,5},{5,4},{6,7},{7,6},{8,9},{9,8},{10,11... | collective-permute-start | bytes 1572872 | tf_op jit(solution)/shard_map/ppermute | solution.py:215
  115.3 2.6 %collective-permute-start.16 = (bf16[1024,256]{1,0:T(8,128)(2,1)S(1)}, bf16[1024,256]{1,0:T(8,128)(2,1)S(1)}, u32[]{:S(2)}, u32[]{:S(2)}) collective-permute-start(bf16[1024,256]{1,0:T(8,128)(2,1)S(1)} %collective-permute-done.10.refs_4_), channel_id=1, source_target_pairs={{0,1},{1,0},{2,3},{3,2},{4,5},{5,4},{6,7},{7,6},{8,9},{9,8},{10,11... | collective-permute-start | bytes 1572872 | tf_op jit(solution)/shard_map/ppermute | solution.py:215
  115.5 13.5 %collective-permute-start.3 = (bf16[1024,256]{1,0:T(8,128)(2,1)S(1)}, bf16[1024,256]{1,0:T(8,128)(2,1)S(1)}, u32[]{:S(2)}, u32[]{:S(2)}) collective-permute-start(bf16[1024,256]{1,0:T(8,128)(2,1)S(1)} %bitcast.14), channel_id=1, source_target_pairs={{0,6},{1,7},{2,0},{3,1},{4,2},{5,3},{6,4},{7,5},{8,14},{9,15},{10,... | collective-permute-start | bytes 1572872 | tf_op jit(solution)/shard_map/ppermute | solution.py:209
  117.1 13.9 %collective-permute-start.4 = (bf16[1024,256]{1,0:T(8,128)(2,1)S(1)}, bf16[1024,256]{1,0:T(8,128)(2,1)S(1)}, u32[]{:S(2)}, u32[]{:S(2)}) collective-permute-start(bf16[1024,256]{1,0:T(8,128)(2,1)S(1)} %bitcast.15), channel_id=1, source_target_pairs={{0,2},{1,3},{2,4},{3,5},{4,6},{5,7},{6,0},{7,1},{8,10},{9,11},{10,... | collective-permute-start | bytes 1572872 | tf_op jit(solution)/shard_map/ppermute | solution.py:212
  117.1 18.5 %collective-permute-start.19 = (bf16[1024,256]{1,0:T(8,128)(2,1)S(1)}, bf16[1024,256]{1,0:T(8,128)(2,1)S(1)}, u32[]{:S(2)}, u32[]{:S(2)}) collective-permute-start(bf16[1024,256]{1,0:T(8,128)(2,1)S(1)} %bitcast.16), channel_id=1, source_target_pairs={{0,1},{1,0},{2,3},{3,2},{4,5},{5,4},{6,7},{7,6},{8,9},{9,8},{10,11... | collective-permute-start | bytes 1572872 | tf_op jit(solution)/shard_map/ppermute | solution.py:215
  117.9 0.8 copy-start.11
  118.7 0.8 copy-start.12
  129.0 6.6 %copy-start.3 = (bf16[1024,256]{1,0:T(8,128)(2,1)}, bf16[1024,256]{1,0:T(8,128)(2,1)S(1)}, u32[]{:S(2)}) copy-start(bf16[1024,256]{1,0:T(8,128)(2,1)S(1)} %collective-permute-done.3.refs_2_) | copy-start | bytes 1572868
  131.0 4.6 %copy-start.4 = (bf16[1024,256]{1,0:T(8,128)(2,1)}, bf16[1024,256]{1,0:T(8,128)(2,1)S(1)}, u32[]{:S(2)}) copy-start(bf16[1024,256]{1,0:T(8,128)(2,1)S(1)} %collective-permute-done.4.refs_4_) | copy-start | bytes 1572868
  131.0 4.6 %collective-permute-start.20 = (bf16[1024,256]{1,0:T(8,128)(2,1)S(1)}, bf16[1024,256]{1,0:T(8,128)(2,1)S(1)}, u32[]{:S(2)}, u32[]{:S(2)}) collective-permute-start(bf16[1024,256]{1,0:T(8,128)(2,1)S(1)} %collective-permute-done.3.refs_2_), channel_id=1, source_target_pairs={{0,1},{1,0},{2,3},{3,2},{4,5},{5,4},{6,7},{7,6},{8,9},{9,8},{10,11... | collective-permute-start | bytes 1572872 | tf_op jit(solution)/shard_map/ppermute | solution.py:215
  132.6 2.9 %collective-permute-start.21 = (bf16[1024,256]{1,0:T(8,128)(2,1)S(1)}, bf16[1024,256]{1,0:T(8,128)(2,1)S(1)}, u32[]{:S(2)}, u32[]{:S(2)}) collective-permute-start(bf16[1024,256]{1,0:T(8,128)(2,1)S(1)} %collective-permute-done.4.refs_4_), channel_id=1, source_target_pairs={{0,1},{1,0},{2,3},{3,2},{4,5},{5,4},{6,7},{7,6},{8,9},{9,8},{10,11... | collective-permute-start | bytes 1572872 | tf_op jit(solution)/shard_map/ppermute | solution.py:215
  134.1 8.1 %collective-permute-start.17 = (bf16[512,256]{1,0:T(8,128)(2,1)}, bf16[512,256]{1,0:T(8,128)(2,1)S(1)}, u32[]{:S(2)}, u32[]{:S(2)}) collective-permute-start(bf16[512,256]{1,0:T(8,128)(2,1)} %slice.26), channel_id=1, source_target_pairs={{0,6},{1,7},{2,0},{3,1},{4,2},{5,3},{6,4},{7,5},{8,14},{9,15},{10,... | collective-permute-start | bytes 786440 | tf_op jit(solution)/shard_map/ppermute | solution.py:209
  134.6 9.0 %collective-permute-start.18 = (bf16[512,256]{1,0:T(8,128)(2,1)}, bf16[512,256]{1,0:T(8,128)(2,1)}, u32[]{:S(2)}, u32[]{:S(2)}) collective-permute-start(bf16[512,256]{1,0:T(8,128)(2,1)} %slice.27), channel_id=1, source_target_pairs={{0,2},{1,3},{2,4},{3,5},{4,6},{5,7},{6,0},{7,1},{8,10},{9,11},{10,... | collective-permute-start | bytes 786440 | tf_op jit(solution)/shard_map/ppermute | solution.py:212
  135.6 0.8 copy-start.5
  135.6 1.0 copy-start.6
  136.5 0.8 copy-start.7
  142.2 4.4 %copy-start.13 = (bf16[512,256]{1,0:T(8,128)(2,1)}, bf16[512,256]{1,0:T(8,128)(2,1)S(1)}, u32[]{:S(2)}) copy-start(bf16[512,256]{1,0:T(8,128)(2,1)S(1)} %collective-permute-done.17.refs_0_) | copy-start | bytes 786436
  143.5 2.4 %collective-permute-start.22 = (bf16[512,256]{1,0:T(8,128)(2,1)S(1)}, bf16[512,256]{1,0:T(8,128)(2,1)S(1)}, u32[]{:S(2)}, u32[]{:S(2)}) collective-permute-start(bf16[512,256]{1,0:T(8,128)(2,1)S(1)} %collective-permute-done.17.refs_0_), channel_id=1, source_target_pairs={{0,1},{1,0},{2,3},{3,2},{4,5},{5,4},{6,7},{7,6},{8,9},{9,8},{10,11... | collective-permute-start | bytes 786440 | tf_op jit(solution)/shard_map/ppermute | solution.py:215
  144.8 1.7 %collective-permute-start.23 = (bf16[512,256]{1,0:T(8,128)(2,1)}, bf16[512,256]{1,0:T(8,128)(2,1)S(1)}, u32[]{:S(2)}, u32[]{:S(2)}) collective-permute-start(bf16[512,256]{1,0:T(8,128)(2,1)} %collective-permute-done.18.refs_1_), channel_id=1, source_target_pairs={{0,1},{1,0},{2,3},{3,2},{4,5},{5,4},{6,7},{7,6},{8,9},{9,8},{10,11... | collective-permute-start | bytes 786440 | tf_op jit(solution)/shard_map/ppermute | solution.py:215
  146.0 0.7 copy-start.14
  146.7 0.7 copy-start.15
where the time goes:
time: 151 us
  blocking collectives  51.5 us (34%)
  Pallas kernels  35.6 us (24%)
  starting transfers between devices  34.7 us (23%)
  waiting for transfers between devices  14.8 us (10%)
  local copies, waits for them, and re-layouts  8.42 us (6%)
  other arithmetic  5.18 us (3%)
    all_gather x1, blocking collectives, work(): packed = lax.all_gather(packed, 'sp', axis=0)  51.5 us
    pallas_call x3, Pallas kernels, conv_blocks(): pl.pallas_call(functools.partial(conv_kernel, counts, first, n_done), out...  27.7 us
    ppermute x13, starting transfers between devices, from_core(): return lax.ppermute(a, 'dp', [(i, i ^ 1) for i in range(n_dp)])  18.1 us
    ppermute x5, starting transfers between devices, from_next(): return lax.ppermute(a, 'dp', [(i, (i - 2) % n_dp) for i in range(n_dp)])  10.3 us
    pallas_call x2, Pallas kernels, out_blocks(): pl.pallas_call(functools.partial(out_kernel, counts, first), out_shape=ja...  7.87 us
    ppermute x5, waiting for transfers between devices, from_last(): return lax.ppermute(a, 'dp', [(i, (i + 2) % n_dp) for i in range(n_dp)])  6.74 us
    unnamed x38, local copies, waits for them, and re-layouts  5.94 us
    ppermute x1, starting transfers between devices, work(): lax.ppermute(tokens[-HALO:], 'sp', [(i, i + 1) for i in range(n_sp - 1)])  5.26 us
  transfers between devices with their start and end apart: 24, of which 8 were waited for; matrix products, arithmetic and copies ran while one was open for 4% of the time, Pallas kernels for 22%

commit v1 on v0

--- a/solution.py
+++ b/solution.py
@@ -12,10 +12,15 @@
 SCALE = 2.0**18
 HALO = 32
 ROWS = 64
+VMEM_LIMIT = 16 * 2**20
 
 
 def whole(space=pltpu.VMEM):
     return pl.BlockSpec(memory_space=space)
+
+
+def near(a):
+    return pltpu.with_memory_space_constraint(a, pltpu.VMEM)
 
 
 def convolve(gated, taps, bias, store, tok_rows):
@@ -44,36 +49,25 @@
     norm = n_done > 0
     if norm:
         (gain_ref, shift_ref), refs = refs[:2], refs[2:]
-    rows_hbm, pieces, refs = refs[0], refs[1 : 1 + n_pieces], refs[1 + n_pieces :]
+    rows, pieces, refs = refs[0], refs[1 : 1 + n_pieces], refs[1 + n_pieces :]
     done, refs = refs[:n_done], refs[n_done:]
     n_outs = 1 if norm else n_blocks
     outs, refs = refs[:n_outs], refs[n_outs:]
-    rows, held, gated, taps_held, sems, conv = refs
+    gated, taps_held, conv = refs
     tok_rows, width = rows.shape[0] - HALO, gated.shape[-1]
     kernel_len = taps_ref.shape[0]
 
-    copies = [pltpu.make_async_copy(rows_hbm, rows, sems.at[0])]
-    at = 0
-    for k, count in enumerate(counts):
-        depth = 0
-        for _ in range(count):
-            size = pieces[at].shape[0]
-            copies.append(pltpu.make_async_copy(pieces[at], held.at[k, pl.ds(depth, size), :], sems.at[1 + at]))
-            depth += size
-            at += 1
-    for k in range(n_done):
-        copies.append(pltpu.make_async_copy(done[k], conv.at[k], sems.at[1 + n_pieces + k]))
-    for copy in copies:
-        copy.start()
-
     def lane_of(k):
         return pl.multiple_of(index_ref[first + k] * width, width)
 
     def project(k):
-        at = 1 + sum(counts[:k])
-        for copy in copies[at : at + counts[k]]:
-            copy.wait()
-        return jnp.dot(rows[...], held[k], preferred_element_type=jnp.float32)
+        at, total = 0, None
+        for piece in pieces[sum(counts[:k]) : sum(counts[: k + 1])]:
+            size = piece.shape[0]
+            part = jnp.dot(rows[:, at : at + size], piece[...], preferred_element_type=jnp.float32)
+            total = part if total is None else total + part
+            at += size
+        return total
 
     def gate(k, both):
         value = both[:, :width].astype(jnp.bfloat16).astype(jnp.float32)
@@ -87,21 +81,18 @@
 
         def store(at, value):
             if norm:
-                conv[n_done + k, pl.ds(at, 8), :] = value
+                conv[k, pl.ds(at, 8), :] = value
             else:
                 outs[k][pl.ds(at, 8), :] = value
 
         convolve(gated.at[k % 2], taps_held.at[k % 2], bias, store, tok_rows)
 
-    copies[0].wait()
     gate(0, project(0))
     for k in range(1, n_blocks):
         both = project(k)
         filter_block(k - 1)
         gate(k, both)
     filter_block(n_blocks - 1)
-    for copy in copies[1 + n_pieces :]:
-        copy.wait()
     if not norm:
         return
 
@@ -111,7 +102,7 @@
 
     def tile(i, carry):
         at = pl.ds(pl.multiple_of(i * 16, 16), 16)
-        values = [conv[k, at, :] for k in range(total)]
+        values = [d[at, :] for d in done] + [conv[k, at, :] for k in range(n_blocks)]
         mean = jnp.sum(sum(values[1:], values[0]), axis=-1, keepdims=True) / (total * width)
         values = [v - mean for v in values]
         squares = [v * v for v in values]
@@ -133,28 +124,26 @@
     n_blocks, n_done = len(blocks), len(done)
     norm = n_done > 0
     if norm:
-        outs = [jax.ShapeDtypeStruct((tok_rows, width * (n_done + n_blocks)), jnp.bfloat16)]
+        outs = [pltpu.VMEM((tok_rows, width * (n_done + n_blocks)), jnp.bfloat16)]
     else:
-        outs = [jax.ShapeDtypeStruct((tok_rows, width), jnp.float32) for _ in blocks]
+        outs = [pltpu.VMEM((tok_rows, width), jnp.float32) for _ in blocks]
     flops = 2 * rows.shape[0] * rows.shape[1] * 2 * width * n_blocks
     return pl.pallas_call(
         functools.partial(conv_kernel, counts, first, n_done),
         out_shape=outs,
         in_specs=[whole(pltpu.SMEM)]
         + [whole()] * (4 if norm else 2)
-        + [whole(pl.ANY)] * (1 + len(pieces) + n_done),
+        + [whole()] * (1 + len(pieces) + n_done),
         out_specs=[whole()] * len(outs),
         scratch_shapes=[
-            pltpu.VMEM(rows.shape, rows.dtype),
-            pltpu.VMEM((n_blocks, rows.shape[1], 2 * width), rows.dtype),
             pltpu.VMEM((2, rows.shape[0], width), jnp.float32),
             pltpu.VMEM((2, taps.shape[0], 8, width), jnp.float32),
-            pltpu.SemaphoreType.DMA((1 + len(pieces) + n_done,)),
-            pltpu.VMEM((n_done + n_blocks, tok_rows, width) if norm else (1, 8, width), jnp.float32),
+            pltpu.VMEM((n_blocks, tok_rows, width) if norm else (1, 8, width), jnp.float32),
         ],
+        compiler_params=pltpu.CompilerParams(vmem_limit_bytes=VMEM_LIMIT),
         cost_estimate=pl.CostEstimate(flops=flops, bytes_accessed=rows.size * 2, transcendentals=0),
         name="conv_norm" if norm else "conv_blocks",
-    )(index, taps, bias, *((gain, shift) if norm else ()), rows, *pieces, *done)
+    )(index, taps, bias, *((gain, shift) if norm else ()), *(near(a) for a in (rows, *pieces, *done)))
 
 
 def out_kernel(counts, first, index_ref, rows_ref, *refs):
@@ -195,9 +184,10 @@
             pltpu.SemaphoreType.DMA((len(blocks),)),
         ],
         input_output_aliases={2 + len(pieces): 0} if more else {},
+        compiler_params=pltpu.CompilerParams(vmem_limit_bytes=VMEM_LIMIT),
         cost_estimate=pl.CostEstimate(flops=2 * rows.size * width * len(blocks), bytes_accessed=rows.size * 6, transcendentals=0),
         name="out_blocks",
-    )(index, rows, *pieces, *more)
+    )(index, *(near(a) for a in (rows, *pieces)), *more)
 
 
 def work(activations, value_weight, gate_weight, conv_taps, conv_bias, norm_gain, norm_bias, out_weight):
@@ -220,7 +210,6 @@
     depth = value_weight.shape[0]
     packed = jnp.concatenate([jnp.concatenate([value_weight, gate_weight], axis=1), out_weight], axis=0)
     packed = (packed.astype(jnp.float32) * SCALE).astype(jnp.float16)
-    packed, halo = hold((packed, halo))
     packed = lax.all_gather(packed, "sp", axis=0)
     packed = (packed.astype(jnp.float32) * (1.0 / SCALE)).astype(jnp.bfloat16)
     width = packed.shape[-1]

time: 151 us -> 140 us (0.927)
  waiting for transfers between devices: 14.8 us -> 32.9 us
  Pallas kernels: 35.6 us -> 19.4 us
  local copies, waits for them, and re-layouts: 8.42 us -> 2.14 us
  starting transfers between devices: 34.7 us -> 29.1 us
    pallas_call x3, Pallas kernels: 27.7 us -> 14.2 us  [conv_blocks(): pl.pallas_call(functools.partial(conv_kernel, counts, first, n_done), out...]
    ppermute x5, waiting for transfers between devices: 6.74 us -> 16.3 us  [from_last(): return lax.ppermute(a, 'dp', [(i, (i + 2) % n_dp) for i in range(n_dp)])]
    ppermute x5, waiting for transfers between devices: 5.21 us -> 11.4 us  [from_next(): return lax.ppermute(a, 'dp', [(i, (i - 2) % n_dp) for i in range(n_dp)])]
    unnamed x38 -> x10, local copies, waits for them, and re-layouts: 5.94 us -> 0.02 us
    ppermute x1, starting transfers between devices: 5.26 us -> 1.31 us  [work(): lax.ppermute(tokens[-HALO:], 'sp', [(i, i + 1) for i in range(n_sp - 1)])]
    pallas_call x2, Pallas kernels: 7.87 us -> 5.29 us  [out_blocks(): pl.pallas_call(functools.partial(out_kernel, counts, first), out_shape=ja...]
    ppermute x13, starting transfers between devices: 18.1 us -> 15.5 us  [from_core(): return lax.ppermute(a, 'dp', [(i, i ^ 1) for i in range(n_dp)])]
    ppermute x1, waiting for transfers between devices: 1.11 us -> 3 us  [work(): lax.ppermute(tokens[-HALO:], 'sp', [(i, i + 1) for i in range(n_sp - 1)])]
  transfers between devices with their start and end apart: 24 -> 24, of which waited for: 8 -> 12; matrix products, arithmetic and copies ran while one was open for 4% -> 3% of each run, Pallas kernels for 22% -> 12%
where the time goes in v1:
time: 140 us
  blocking collectives  52.4 us (37%)
  waiting for transfers between devices  32.9 us (24%)
  starting transfers between devices  29.1 us (21%)
  Pallas kernels  19.4 us (14%)
  other arithmetic  3.75 us (3%)
  local copies, waits for them, and re-layouts  2.14 us (2%)
    all_gather x1, blocking collectives, work(): packed = lax.all_gather(packed, 'sp', axis=0)  52.4 us
    ppermute x5, waiting for transfers between devices, from_last(): return lax.ppermute(a, 'dp', [(i, (i + 2) % n_dp) for i in range(n_dp)])  16.3 us
    ppermute x13, starting transfers between devices, from_core(): return lax.ppermute(a, 'dp', [(i, i ^ 1) for i in range(n_dp)])  15.5 us
    pallas_call x3, Pallas kernels, conv_blocks(): pl.pallas_call(functools.partial(conv_kernel, counts, first, n_done), out...  14.2 us
    ppermute x5, waiting for transfers between devices, from_next(): return lax.ppermute(a, 'dp', [(i, (i - 2) % n_dp) for i in range(n_dp)])  11.4 us
    ppermute x5, starting transfers between devices, from_next(): return lax.ppermute(a, 'dp', [(i, (i - 2) % n_dp) for i in range(n_dp)])  10.8 us
    pallas_call x2, Pallas kernels, out_blocks(): pl.pallas_call(functools.partial(out_kernel, counts, first), out_shape=ja...  5.29 us
    ppermute x1, waiting for transfers between devices, work(): lax.ppermute(tokens[-HALO:], 'sp', [(i, i + 1) for i in range(n_sp - 1)])  3 us
  transfers between devices with their start and end apart: 24, of which 12 were waited for; matrix products, arithmetic and copies ran while one was open for 3% of the time, Pallas kernels for 12%

profile of v1, /device:TPU:33, one launch (start us, length us, event | category | flops | bytes accessed | tf_op | source)
XLA Modules:
  0.0 140.0 jit_solution(1708420419934741273)
XLA Ops:
  0.0 0.8 maximum_bitcast_fusion
  0.8 0.8 multiply_convert_fusion.1
  1.6 52.4 %all-gather.1 = f16[16,192,256]{2,1,0:T(8,128)(2,1)S(1)} all-gather(f16[1,192,256]{2,1,0:T(8,128)(2,1)S(1)} %multiply_convert_fusion.1), channel_id=1, replica_groups=mesh['grp'=2,'sp'=16,'dp'=8] {'sp'}, dimensions={0}, use_global_device_ids=true | all-gather | bytes 1671168 | tf_op jit(solution)/shard_map/all_gather | solution.py:213
  53.9 0.4 multiply_convert_fusion
  54.3 0.0 copy-start.4
  54.3 0.1 fusion.3
  54.4 7.4 %collective-permute-start.7 = (bf16[1024,256]{1,0:T(8,128)(2,1)S(1)}, bf16[1024,256]{1,0:T(8,128)(2,1)S(1)}, u32[]{:S(2)}, u32[]{:S(2)}) collective-permute-start(bf16[1024,256]{1,0:T(8,128)(2,1)S(1)} %bitcast.17), channel_id=1, source_target_pairs={{0,1},{1,0},{2,3},{3,2},{4,5},{5,4},{6,7},{7,6},{8,9},{9,8},{10,11... | collective-permute-start | bytes 1572872 | tf_op jit(solution)/shard_map/ppermute | solution.py:205
  61.8 2.9 %collective-permute-start.5 = (bf16[1024,256]{1,0:T(8,128)(2,1)S(1)}, bf16[1024,256]{1,0:T(8,128)(2,1)S(1)}, u32[]{:S(2)}, u32[]{:S(2)}) collective-permute-start(bf16[1024,256]{1,0:T(8,128)(2,1)S(1)} %bitcast.18), channel_id=1, source_target_pairs={{0,6},{1,7},{2,0},{3,1},{4,2},{5,3},{6,4},{7,5},{8,14},{9,15},{10,... | collective-permute-start | bytes 1572872 | tf_op jit(solution)/shard_map/ppermute | solution.py:199
  64.7 0.0 copy-done.4
  64.7 0.4 collective-permute-start.8
  65.1 0.0 collective-permute-start.6
  65.1 0.9 slice_bitcast_fusion
  66.0 1.3 collective-permute-start.4
  67.4 3.0 %collective-permute-done.4 = bf16[32,2048]{1,0:T(8,128)(2,1)S(1)} collective-permute-done((bf16[32,2048]{1,0:T(8,128)(2,1)S(1)}, bf16[32,2048]{1,0:T(8,128)(2,1)S(1)}, u32[]{:S(2)}, u32[]{:S(2)}) %collective-permute-start.4) | collective-permute-done | bytes 131104 | tf_op jit(solution)/shard_map/ppermute | solution.py:207
  70.4 2.4 %collective-permute-start = (bf16[1024,256]{1,0:T(8,128)(2,1)S(1)}, bf16[1024,256]{1,0:T(8,128)(2,1)S(1)}, u32[]{:S(2)}, u32[]{:S(2)}) collective-permute-start(bf16[1024,256]{1,0:T(8,128)(2,1)S(1)} %bitcast.23), channel_id=1, source_target_pairs={{0,6},{1,7},{2,0},{3,1},{4,2},{5,3},{6,4},{7,5},{8,14},{9,15},{10,... | collective-permute-start | bytes 1572872 | tf_op jit(solution)/shard_map/ppermute | solution.py:199
  72.8 0.0 collective-permute-done.7.refs_3_
  72.8 0.0 collective-permute-start.1
  72.8 0.0 copy-start.1
  72.8 1.8 %pad_maximum_fusion.refs_0_.refs_2_ = bf16[544,2048]{1,0:T(8,128)(2,1)S(1)} fusion(bf16[512,2048]{1,0:T(8,128)(2,1)} %bitcast.30, bf16[32,2048]{1,0:T(8,128)(2,1)S(1)} %collective-permute-done.4), kind=kLoop, calls=%fused_computation.1 | loop fusion | flops 4456448 | bytes 4456448 | tf_op jit(solution)/shard_map/concatenate | solution.py:228
  74.6 0.0 collective-permute-done.8.refs_4_
  74.6 3.2 %conv_blocks.2 = (f32[512,128]{1,0:T(8,128)S(1)}, f32[512,128]{1,0:T(8,128)S(1)}) custom-call(s32[8]{0:T(128)S(1)} %fusion.index_ref, f32[31,1024]{1,0:T(8,128)S(1)} %copy-done, f32[1,1024]{1,0:T(1,128)S(1)} %bitcast.25, bf16[544,2048]{1,0:T(8,128)(2,1)S(1)} %pad_maximum_fusion.refs_0_.refs_2_, bf16[1024,256]{1,0:T(8,128)(2,1)S(1)} %bitcast.20, ...), custom_call_target="tpu_custom_call" | custom-call | flops 1140850688 | bytes 2228224 | tf_op jit(solution)/shard_map/conv_blocks/pallas_call | solution.py:131
  77.8 0.0 collective-permute-done.5.refs_1_
  77.8 1.9 %collective-permute-done.6.refs_6_ = bf16[1024,256]{1,0:T(8,128)(2,1)S(1)} collective-permute-done((bf16[1024,256]{1,0:T(8,128)(2,1)S(1)}, bf16[1024,256]{1,0:T(8,128)(2,1)S(1)}, u32[]{:S(2)}, u32[]{:S(2)}) %collective-permute-start.6) | collective-permute-done | bytes 524320 | tf_op jit(solution)/shard_map/ppermute | solution.py:202
  79.7 1.5 %collective-permute-start.11 = (bf16[1024,256]{1,0:T(8,128)(2,1)S(1)}, bf16[1024,256]{1,0:T(8,128)(2,1)S(1)}, u32[]{:S(2)}, u32[]{:S(2)}) collective-permute-start(bf16[1024,256]{1,0:T(8,128)(2,1)S(1)} %collective-permute-done.5.refs_1_), channel_id=1, source_target_pairs={{0,1},{1,0},{2,3},{3,2},{4,5},{5,4},{6,7},{7,6},{8,9},{9,8},{10,11... | collective-permute-start | bytes 1572872 | tf_op jit(solution)/shard_map/ppermute | solution.py:205
  81.2 1.1 slice.30
  82.3 0.1 collective-permute-start.14
  82.4 4.6 %collective-permute-done.refs_2_ = bf16[1024,256]{1,0:T(8,128)(2,1)S(1)} collective-permute-done((bf16[1024,256]{1,0:T(8,128)(2,1)S(1)}, bf16[1024,256]{1,0:T(8,128)(2,1)S(1)}, u32[]{:S(2)}, u32[]{:S(2)}) %collective-permute-start) | collective-permute-done | bytes 524320 | tf_op jit(solution)/shard_map/ppermute | solution.py:199
  87.1 3.9 %collective-permute-done.1.refs_5_ = bf16[1024,256]{1,0:T(8,128)(2,1)S(1)} collective-permute-done((bf16[1024,256]{1,0:T(8,128)(2,1)S(1)}, bf16[1024,256]{1,0:T(8,128)(2,1)S(1)}, u32[]{:S(2)}, u32[]{:S(2)}) %collective-permute-start.1) | collective-permute-done | bytes 524320 | tf_op jit(solution)/shard_map/ppermute | solution.py:202
  90.9 0.9 collective-permute-start.12
  91.9 0.1 collective-permute-start.13
  92.0 0.0 collective-permute-start.10
  92.0 0.0 collective-permute-done.11.refs_3_
  92.0 2.7 %collective-permute-start.9 = (bf16[1024,256]{1,0:T(8,128)(2,1)S(1)}, bf16[1024,256]{1,0:T(8,128)(2,1)S(1)}, u32[]{:S(2)}, u32[]{:S(2)}) collective-permute-start(bf16[1024,256]{1,0:T(8,128)(2,1)S(1)} %collective-permute-done.5.refs_1_), channel_id=1, source_target_pairs={{0,6},{1,7},{2,0},{3,1},{4,2},{5,3},{6,4},{7,5},{8,14},{9,15},{10,... | collective-permute-start | bytes 1572872 | tf_op jit(solution)/shard_map/ppermute | solution.py:199
  94.7 0.0 collective-permute-done.14.refs_8_
  94.7 0.0 collective-permute-done.12.refs_4_
  94.7 0.0 collective-permute-done.13.refs_7_
  94.7 5.8 %conv_blocks.3 = (f32[512,128]{1,0:T(8,128)S(1)}, f32[512,128]{1,0:T(8,128)S(1)}, f32[512,128]{1,0:T(8,128)S(1)}, f32[512,128]{1,0:T(8,128)S(1)}) custom-call(s32[8]{0:T(128)S(1)} %fusion.index_ref, f32[31,1024]{1,0:T(8,128)S(1)} %copy-done, f32[1,1024]{1,0:T(1,128)S(1)} %bitcast.26, bf16[544,2048]{1,0:T(8,128)(2,1)S(1)} %pad_maximum_fusion.refs_0_.refs_2_, ...), custom_call_target="tpu_custom_call" | custom-call | flops 2281701376 | bytes 2228224 | tf_op jit(solution)/shard_map/conv_blocks/pallas_call | solution.py:131
  100.5 5.8 %collective-permute-done.10.refs_4_ = bf16[1024,256]{1,0:T(8,128)(2,1)S(1)} collective-permute-done((bf16[1024,256]{1,0:T(8,128)(2,1)S(1)}, bf16[1024,256]{1,0:T(8,128)(2,1)S(1)}, u32[]{:S(2)}, u32[]{:S(2)}) %collective-permute-start.10) | collective-permute-done | bytes 524320 | tf_op jit(solution)/shard_map/ppermute | solution.py:202
  106.3 0.0 collective-permute-done.9.refs_3_
  106.3 1.2 collective-permute-start.15
  107.6 0.0 collective-permute-start.16
  107.6 2.7 %collective-permute-start.2 = (bf16[1024,256]{1,0:T(8,128)(2,1)S(1)}, bf16[1024,256]{1,0:T(8,128)(2,1)S(1)}, u32[]{:S(2)}, u32[]{:S(2)}) collective-permute-start(bf16[1024,256]{1,0:T(8,128)(2,1)S(1)} %bitcast.13), channel_id=1, source_target_pairs={{0,6},{1,7},{2,0},{3,1},{4,2},{5,3},{6,4},{7,5},{8,14},{9,15},{10,... | collective-permute-start | bytes 1572872 | tf_op jit(solution)/shard_map/ppermute | solution.py:199
  110.3 0.0 collective-permute-start.3
  110.3 0.8 collective-permute-start.19
  111.0 0.0 collective-permute-done.15.refs_5_
  111.0 0.0 collective-permute-done.16.refs_6_
  111.1 5.2 %conv_norm.1.rows_ref = bf16[512,1024]{1,0:T(8,128)(2,1)S(1)} custom-call(s32[8]{0:T(128)S(1)} %fusion.index_ref, f32[31,1024]{1,0:T(8,128)S(1)} %copy-done, f32[1,1024]{1,0:T(1,128)S(1)} %bitcast.27, f32[1,1024]{1,0:T(1,128)S(1)} %bitcast.28, f32[1,1024]{1,0:T(1,128)S(1)} %bitcast.29, bf16[544,2048]{1,0:T(8,128)(2,1)S(1)} %pad_maximum_fusion.refs_0_.refs_2_, ...), custom_call_target="tpu_custom_call" | custom-call | flops 1140850688 | bytes 2228224 | tf_op jit(solution)/shard_map/conv_norm/pallas_call | solution.py:131
  116.3 4.7 %collective-permute-done.2.refs_2_ = bf16[1024,256]{1,0:T(8,128)(2,1)S(1)} collective-permute-done((bf16[1024,256]{1,0:T(8,128)(2,1)S(1)}, bf16[1024,256]{1,0:T(8,128)(2,1)S(1)}, u32[]{:S(2)}, u32[]{:S(2)}) %collective-permute-start.2) | collective-permute-done | bytes 524320 | tf_op jit(solution)/shard_map/ppermute | solution.py:199
  121.0 3.1 %collective-permute-done.3.refs_4_ = bf16[1024,256]{1,0:T(8,128)(2,1)S(1)} collective-permute-done((bf16[1024,256]{1,0:T(8,128)(2,1)S(1)}, bf16[1024,256]{1,0:T(8,128)(2,1)S(1)}, u32[]{:S(2)}, u32[]{:S(2)}) %collective-permute-start.3) | collective-permute-done | bytes 524320 | tf_op jit(solution)/shard_map/ppermute | solution.py:202
  124.2 1.6 %collective-permute-start.20 = (bf16[1024,256]{1,0:T(8,128)(2,1)S(1)}, bf16[1024,256]{1,0:T(8,128)(2,1)S(1)}, u32[]{:S(2)}, u32[]{:S(2)}) collective-permute-start(bf16[1024,256]{1,0:T(8,128)(2,1)S(1)} %collective-permute-done.2.refs_2_), channel_id=1, source_target_pairs={{0,1},{1,0},{2,3},{3,2},{4,5},{5,4},{6,7},{7,6},{8,9},{9,8},{10,11... | collective-permute-start | bytes 1572872 | tf_op jit(solution)/shard_map/ppermute | solution.py:205
  125.8 0.0 collective-permute-start.21
  125.9 0.1 collective-permute-start.17
  126.0 1.4 %collective-permute-start.18 = (bf16[512,256]{1,0:T(8,128)(2,1)S(1)}, bf16[512,256]{1,0:T(8,128)(2,1)S(1)}, u32[]{:S(2)}, u32[]{:S(2)}) collective-permute-start(bf16[512,256]{1,0:T(8,128)(2,1)S(1)} %slice.27), channel_id=1, source_target_pairs={{0,2},{1,3},{2,4},{3,5},{4,6},{5,7},{6,0},{7,1},{8,10},{9,11},{10,... | collective-permute-start | bytes 786440 | tf_op jit(solution)/shard_map/ppermute | solution.py:202
  127.4 0.0 collective-permute-done.19.refs_1_
  127.4 0.0 collective-permute-done.20.refs_3_
  127.4 0.6 collective-permute-done.21.refs_5_
  128.1 3.2 %out_blocks.2.refs_4_ = bf16[512,2048]{1,0:T(8,128)(2,1)} custom-call(s32[8]{0:T(128)S(1)} %fusion.index_ref, bf16[512,1024]{1,0:T(8,128)(2,1)S(1)} %conv_norm.1.rows_ref, bf16[1024,256]{1,0:T(8,128)(2,1)S(1)} %bitcast.16, bf16[1024,256]{1,0:T(8,128)(2,1)S(1)} %collective-permute-done.19.refs_1_, bf16[1024,256]{1,0:T(8,128)(2,1)S(1)} %collective-permute-done.2.refs_2_, ...), custom_call_target="tpu_custom_call" | custom-call | flops 1610612736 | bytes 3145728 | tf_op jit(solution)/shard_map/out_blocks/pallas_call | solution.py:177
  131.3 2.0 %collective-permute-done.17.refs_0_ = bf16[512,256]{1,0:T(8,128)(2,1)S(1)} collective-permute-done((bf16[512,256]{1,0:T(8,128)(2,1)S(1)}, bf16[512,256]{1,0:T(8,128)(2,1)S(1)}, u32[]{:S(2)}, u32[]{:S(2)}) %collective-permute-start.17) | collective-permute-done | bytes 262176 | tf_op jit(solution)/shard_map/ppermute | solution.py:199
  133.3 1.6 %collective-permute-done.18.refs_1_ = bf16[512,256]{1,0:T(8,128)(2,1)S(1)} collective-permute-done((bf16[512,256]{1,0:T(8,128)(2,1)S(1)}, bf16[512,256]{1,0:T(8,128)(2,1)S(1)}, u32[]{:S(2)}, u32[]{:S(2)}) %collective-permute-start.18) | collective-permute-done | bytes 262176 | tf_op jit(solution)/shard_map/ppermute | solution.py:202
  134.9 1.4 collective-permute-start.22
  136.3 0.0 collective-permute-start.23
  136.3 1.2 collective-permute-done.22.refs_2_
  137.4 0.4 collective-permute-done.23.refs_3_
  137.8 2.1 %out_blocks.3 = bf16[512,2048]{1,0:T(8,128)(2,1)} custom-call(s32[8]{0:T(128)S(1)} %fusion.index_ref, bf16[512,1024]{1,0:T(8,128)(2,1)S(1)} %conv_norm.1.rows_ref, bf16[512,256]{1,0:T(8,128)(2,1)S(1)} %collective-permute-done.17.refs_0_, bf16[512,256]{1,0:T(8,128)(2,1)S(1)} %collective-permute-done.18.refs_1_, ...), custom_call_target="tpu_custom_call", output_to_operand_aliasing={{}: (6, {})} | custom-call | flops 536870912 | bytes 3145728 | tf_op jit(solution)/shard_map/out_blocks/pallas_call | solution.py:177
  (10 shorter events, 0.1 us)
Async XLA Ops:
  54.3 10.4 %copy-start.4 = (bf16[16,192,256]{2,1,0:T(8,128)(2,1)}, bf16[16,192,256]{2,1,0:T(8,128)(2,1)S(1)}, u32[]{:S(2)}) copy-start(bf16[16,192,256]{2,1,0:T(8,128)(2,1)S(1)} %multiply_convert_fusion) | copy-start | bytes 4718596
  54.4 18.3 %collective-permute-start.7 = (bf16[1024,256]{1,0:T(8,128)(2,1)S(1)}, bf16[1024,256]{1,0:T(8,128)(2,1)S(1)}, u32[]{:S(2)}, u32[]{:S(2)}) collective-permute-start(bf16[1024,256]{1,0:T(8,128)(2,1)S(1)} %bitcast.17), channel_id=1, source_target_pairs={{0,1},{1,0},{2,3},{3,2},{4,5},{5,4},{6,7},{7,6},{8,9},{9,8},{10,11... | collective-permute-start | bytes 1572872 | tf_op jit(solution)/shard_map/ppermute | solution.py:205
  61.8 16.0 %collective-permute-start.5 = (bf16[1024,256]{1,0:T(8,128)(2,1)S(1)}, bf16[1024,256]{1,0:T(8,128)(2,1)S(1)}, u32[]{:S(2)}, u32[]{:S(2)}) collective-permute-start(bf16[1024,256]{1,0:T(8,128)(2,1)S(1)} %bitcast.18), channel_id=1, source_target_pairs={{0,6},{1,7},{2,0},{3,1},{4,2},{5,3},{6,4},{7,5},{8,14},{9,15},{10,... | collective-permute-start | bytes 1572872 | tf_op jit(solution)/shard_map/ppermute | solution.py:199
  64.7 9.9 %collective-permute-start.8 = (bf16[1024,256]{1,0:T(8,128)(2,1)S(1)}, bf16[1024,256]{1,0:T(8,128)(2,1)S(1)}, u32[]{:S(2)}, u32[]{:S(2)}) collective-permute-start(bf16[1024,256]{1,0:T(8,128)(2,1)S(1)} %bitcast.21), channel_id=1, source_target_pairs={{0,1},{1,0},{2,3},{3,2},{4,5},{5,4},{6,7},{7,6},{8,9},{9,8},{10,11... | collective-permute-start | bytes 1572872 | tf_op jit(solution)/shard_map/ppermute | solution.py:205
  65.1 14.6 %collective-permute-start.6 = (bf16[1024,256]{1,0:T(8,128)(2,1)S(1)}, bf16[1024,256]{1,0:T(8,128)(2,1)S(1)}, u32[]{:S(2)}, u32[]{:S(2)}) collective-permute-start(bf16[1024,256]{1,0:T(8,128)(2,1)S(1)} %bitcast.22), channel_id=1, source_target_pairs={{0,2},{1,3},{2,4},{3,5},{4,6},{5,7},{6,0},{7,1},{8,10},{9,11},{10,... | collective-permute-start | bytes 1572872 | tf_op jit(solution)/shard_map/ppermute | solution.py:202
  66.0 4.3 %collective-permute-start.4 = (bf16[32,2048]{1,0:T(8,128)(2,1)S(1)}, bf16[32,2048]{1,0:T(8,128)(2,1)S(1)}, u32[]{:S(2)}, u32[]{:S(2)}) collective-permute-start(bf16[32,2048]{1,0:T(8,128)(2,1)S(1)} %slice_bitcast_fusion), channel_id=1, source_target_pairs={{0,8},{8,16},{16,24},{24,32},{32,40},{40,48},{48,56},{56,64},{64,7... | collective-permute-start | bytes 393224 | tf_op jit(solution)/shard_map/ppermute | solution.py:207
  70.4 16.7 %collective-permute-start = (bf16[1024,256]{1,0:T(8,128)(2,1)S(1)}, bf16[1024,256]{1,0:T(8,128)(2,1)S(1)}, u32[]{:S(2)}, u32[]{:S(2)}) collective-permute-start(bf16[1024,256]{1,0:T(8,128)(2,1)S(1)} %bitcast.23), channel_id=1, source_target_pairs={{0,6},{1,7},{2,0},{3,1},{4,2},{5,3},{6,4},{7,5},{8,14},{9,15},{10,... | collective-permute-start | bytes 1572872 | tf_op jit(solution)/shard_map/ppermute | solution.py:199
  72.8 18.2 %collective-permute-start.1 = (bf16[1024,256]{1,0:T(8,128)(2,1)S(1)}, bf16[1024,256]{1,0:T(8,128)(2,1)S(1)}, u32[]{:S(2)}, u32[]{:S(2)}) collective-permute-start(bf16[1024,256]{1,0:T(8,128)(2,1)S(1)} %bitcast.19), channel_id=1, source_target_pairs={{0,2},{1,3},{2,4},{3,5},{4,6},{5,7},{6,0},{7,1},{8,10},{9,11},{10,... | collective-permute-start | bytes 1572872 | tf_op jit(solution)/shard_map/ppermute | solution.py:202
  72.8 1.8 %copy-start = (f32[31,1024]{1,0:T(8,128)S(1)}, f32[31,1024]{1,0:T(8,128)}, u32[]{:S(2)}) copy-start(f32[31,1024]{1,0:T(8,128)} %taps_ref.5) | copy-start | bytes 380932
  72.8 1.8 %copy-start.1 = (f32[1024]{0:T(1024)S(1)}, f32[1024]{0:T(1024)}, u32[]{:S(2)}) copy-start(f32[1024]{0:T(1024)} %param.12) | copy-start | bytes 12292
  79.7 12.3 %collective-permute-start.11 = (bf16[1024,256]{1,0:T(8,128)(2,1)S(1)}, bf16[1024,256]{1,0:T(8,128)(2,1)S(1)}, u32[]{:S(2)}, u32[]{:S(2)}) collective-permute-start(bf16[1024,256]{1,0:T(8,128)(2,1)S(1)} %collective-permute-done.5.refs_1_), channel_id=1, source_target_pairs={{0,1},{1,0},{2,3},{3,2},{4,5},{5,4},{6,7},{7,6},{8,9},{9,8},{10,11... | collective-permute-start | bytes 1572872 | tf_op jit(solution)/shard_map/ppermute | solution.py:205
  82.3 12.4 %collective-permute-start.14 = (bf16[1024,256]{1,0:T(8,128)(2,1)S(1)}, bf16[1024,256]{1,0:T(8,128)(2,1)S(1)}, u32[]{:S(2)}, u32[]{:S(2)}) collective-permute-start(bf16[1024,256]{1,0:T(8,128)(2,1)S(1)} %collective-permute-done.6.refs_6_), channel_id=1, source_target_pairs={{0,1},{1,0},{2,3},{3,2},{4,5},{5,4},{6,7},{7,6},{8,9},{9,8},{10,11... | collective-permute-start | bytes 1572872 | tf_op jit(solution)/shard_map/ppermute | solution.py:205
  90.9 20.1 %copy-start.2 = (f32[1024]{0:T(1024)S(1)}, f32[1024]{0:T(1024)}, u32[]{:S(2)}) copy-start(f32[1024]{0:T(1024)} %param.13) | copy-start | bytes 12292
  90.9 20.1 %copy-start.3 = (f32[1024]{0:T(1024)S(1)}, f32[1024]{0:T(1024)}, u32[]{:S(2)}) copy-start(f32[1024]{0:T(1024)} %param.14) | copy-start | bytes 12292
  90.9 3.8 %collective-permute-start.12 = (bf16[1024,256]{1,0:T(8,128)(2,1)S(1)}, bf16[1024,256]{1,0:T(8,128)(2,1)S(1)}, u32[]{:S(2)}, u32[]{:S(2)}) collective-permute-start(bf16[1024,256]{1,0:T(8,128)(2,1)S(1)} %collective-permute-done.refs_2_), channel_id=1, source_target_pairs={{0,1},{1,0},{2,3},{3,2},{4,5},{5,4},{6,7},{7,6},{8,9},{9,8},{10,11... | collective-permute-start | bytes 1572872 | tf_op jit(solution)/shard_map/ppermute | solution.py:205
  91.9 2.8 %collective-permute-start.13 = (bf16[1024,256]{1,0:T(8,128)(2,1)S(1)}, bf16[1024,256]{1,0:T(8,128)(2,1)S(1)}, u32[]{:S(2)}, u32[]{:S(2)}) collective-permute-start(bf16[1024,256]{1,0:T(8,128)(2,1)S(1)} %collective-permute-done.1.refs_5_), channel_id=1, source_target_pairs={{0,1},{1,0},{2,3},{3,2},{4,5},{5,4},{6,7},{7,6},{8,9},{9,8},{10,11... | collective-permute-start | bytes 1572872 | tf_op jit(solution)/shard_map/ppermute | solution.py:205
  92.0 14.3 %collective-permute-start.10 = (bf16[1024,256]{1,0:T(8,128)(2,1)S(1)}, bf16[1024,256]{1,0:T(8,128)(2,1)S(1)}, u32[]{:S(2)}, u32[]{:S(2)}) collective-permute-start(bf16[1024,256]{1,0:T(8,128)(2,1)S(1)} %collective-permute-done.6.refs_6_), channel_id=1, source_target_pairs={{0,2},{1,3},{2,4},{3,5},{4,6},{5,7},{6,0},{7,1},{8,10},{9,11},{10,... | collective-permute-start | bytes 1572872 | tf_op jit(solution)/shard_map/ppermute | solution.py:202
  92.0 14.3 %collective-permute-start.9 = (bf16[1024,256]{1,0:T(8,128)(2,1)S(1)}, bf16[1024,256]{1,0:T(8,128)(2,1)S(1)}, u32[]{:S(2)}, u32[]{:S(2)}) collective-permute-start(bf16[1024,256]{1,0:T(8,128)(2,1)S(1)} %collective-permute-done.5.refs_1_), channel_id=1, source_target_pairs={{0,6},{1,7},{2,0},{3,1},{4,2},{5,3},{6,4},{7,5},{8,14},{9,15},{10,... | collective-permute-start | bytes 1572872 | tf_op jit(solution)/shard_map/ppermute | solution.py:199
  106.3 4.7 %collective-permute-start.15 = (bf16[1024,256]{1,0:T(8,128)(2,1)S(1)}, bf16[1024,256]{1,0:T(8,128)(2,1)S(1)}, u32[]{:S(2)}, u32[]{:S(2)}) collective-permute-start(bf16[1024,256]{1,0:T(8,128)(2,1)S(1)} %collective-permute-done.9.refs_3_), channel_id=1, source_target_pairs={{0,1},{1,0},{2,3},{3,2},{4,5},{5,4},{6,7},{7,6},{8,9},{9,8},{10,11... | collective-permute-start | bytes 1572872 | tf_op jit(solution)/shard_map/ppermute | solution.py:205
  107.6 3.5 %collective-permute-start.16 = (bf16[1024,256]{1,0:T(8,128)(2,1)S(1)}, bf16[1024,256]{1,0:T(8,128)(2,1)S(1)}, u32[]{:S(2)}, u32[]{:S(2)}) collective-permute-start(bf16[1024,256]{1,0:T(8,128)(2,1)S(1)} %collective-permute-done.10.refs_4_), channel_id=1, source_target_pairs={{0,1},{1,0},{2,3},{3,2},{4,5},{5,4},{6,7},{7,6},{8,9},{9,8},{10,11... | collective-permute-start | bytes 1572872 | tf_op jit(solution)/shard_map/ppermute | solution.py:205
  107.6 13.4 %collective-permute-start.2 = (bf16[1024,256]{1,0:T(8,128)(2,1)S(1)}, bf16[1024,256]{1,0:T(8,128)(2,1)S(1)}, u32[]{:S(2)}, u32[]{:S(2)}) collective-permute-start(bf16[1024,256]{1,0:T(8,128)(2,1)S(1)} %bitcast.13), channel_id=1, source_target_pairs={{0,6},{1,7},{2,0},{3,1},{4,2},{5,3},{6,4},{7,5},{8,14},{9,15},{10,... | collective-permute-start | bytes 1572872 | tf_op jit(solution)/shard_map/ppermute | solution.py:199
  110.3 13.9 %collective-permute-start.3 = (bf16[1024,256]{1,0:T(8,128)(2,1)S(1)}, bf16[1024,256]{1,0:T(8,128)(2,1)S(1)}, u32[]{:S(2)}, u32[]{:S(2)}) collective-permute-start(bf16[1024,256]{1,0:T(8,128)(2,1)S(1)} %bitcast.14), channel_id=1, source_target_pairs={{0,2},{1,3},{2,4},{3,5},{4,6},{5,7},{6,0},{7,1},{8,10},{9,11},{10,... | collective-permute-start | bytes 1572872 | tf_op jit(solution)/shard_map/ppermute | solution.py:202
  110.3 17.2 %collective-permute-start.19 = (bf16[1024,256]{1,0:T(8,128)(2,1)S(1)}, bf16[1024,256]{1,0:T(8,128)(2,1)S(1)}, u32[]{:S(2)}, u32[]{:S(2)}) collective-permute-start(bf16[1024,256]{1,0:T(8,128)(2,1)S(1)} %bitcast.15), channel_id=1, source_target_pairs={{0,1},{1,0},{2,3},{3,2},{4,5},{5,4},{6,7},{7,6},{8,9},{9,8},{10,11... | collective-permute-start | bytes 1572872 | tf_op jit(solution)/shard_map/ppermute | solution.py:205
  124.2 3.3 %collective-permute-start.20 = (bf16[1024,256]{1,0:T(8,128)(2,1)S(1)}, bf16[1024,256]{1,0:T(8,128)(2,1)S(1)}, u32[]{:S(2)}, u32[]{:S(2)}) collective-permute-start(bf16[1024,256]{1,0:T(8,128)(2,1)S(1)} %collective-permute-done.2.refs_2_), channel_id=1, source_target_pairs={{0,1},{1,0},{2,3},{3,2},{4,5},{5,4},{6,7},{7,6},{8,9},{9,8},{10,11... | collective-permute-start | bytes 1572872 | tf_op jit(solution)/shard_map/ppermute | solution.py:205
  125.8 2.3 %collective-permute-start.21 = (bf16[1024,256]{1,0:T(8,128)(2,1)S(1)}, bf16[1024,256]{1,0:T(8,128)(2,1)S(1)}, u32[]{:S(2)}, u32[]{:S(2)}) collective-permute-start(bf16[1024,256]{1,0:T(8,128)(2,1)S(1)} %collective-permute-done.3.refs_4_), channel_id=1, source_target_pairs={{0,1},{1,0},{2,3},{3,2},{4,5},{5,4},{6,7},{7,6},{8,9},{9,8},{10,11... | collective-permute-start | bytes 1572872 | tf_op jit(solution)/shard_map/ppermute | solution.py:205
  125.9 7.5 %collective-permute-start.17 = (bf16[512,256]{1,0:T(8,128)(2,1)S(1)}, bf16[512,256]{1,0:T(8,128)(2,1)S(1)}, u32[]{:S(2)}, u32[]{:S(2)}) collective-permute-start(bf16[512,256]{1,0:T(8,128)(2,1)S(1)} %slice.26), channel_id=1, source_target_pairs={{0,6},{1,7},{2,0},{3,1},{4,2},{5,3},{6,4},{7,5},{8,14},{9,15},{10,... | collective-permute-start | bytes 786440 | tf_op jit(solution)/shard_map/ppermute | solution.py:199
  126.0 8.9 %collective-permute-start.18 = (bf16[512,256]{1,0:T(8,128)(2,1)S(1)}, bf16[512,256]{1,0:T(8,128)(2,1)S(1)}, u32[]{:S(2)}, u32[]{:S(2)}) collective-permute-start(bf16[512,256]{1,0:T(8,128)(2,1)S(1)} %slice.27), channel_id=1, source_target_pairs={{0,2},{1,3},{2,4},{3,5},{4,6},{5,7},{6,0},{7,1},{8,10},{9,11},{10,... | collective-permute-start | bytes 786440 | tf_op jit(solution)/shard_map/ppermute | solution.py:202
  134.9 2.5 %collective-permute-start.22 = (bf16[512,256]{1,0:T(8,128)(2,1)S(1)}, bf16[512,256]{1,0:T(8,128)(2,1)S(1)}, u32[]{:S(2)}, u32[]{:S(2)}) collective-permute-start(bf16[512,256]{1,0:T(8,128)(2,1)S(1)} %collective-permute-done.17.refs_0_), channel_id=1, source_target_pairs={{0,1},{1,0},{2,3},{3,2},{4,5},{5,4},{6,7},{7,6},{8,9},{9,8},{10,11... | collective-permute-start | bytes 786440 | tf_op jit(solution)/shard_map/ppermute | solution.py:205
  136.3 1.5 %collective-permute-start.23 = (bf16[512,256]{1,0:T(8,128)(2,1)S(1)}, bf16[512,256]{1,0:T(8,128)(2,1)S(1)}, u32[]{:S(2)}, u32[]{:S(2)}) collective-permute-start(bf16[512,256]{1,0:T(8,128)(2,1)S(1)} %collective-permute-done.18.refs_1_), channel_id=1, source_target_pairs={{0,1},{1,0},{2,3},{3,2},{4,5},{5,4},{6,7},{7,6},{8,9},{9,8},{10,11... | collective-permute-start | bytes 786440 | tf_op jit(solution)/shard_map/ppermute | solution.py:205

commit v2 on v1

--- a/solution.py
+++ b/solution.py
@@ -216,42 +216,54 @@
     upper = packed[: n_sp // 2, :depth].reshape(-1, width)
     lower = packed[n_sp // 2 :, :depth].reshape(-1, width)
     o_own = packed[:, depth:].reshape(-1, width)
+    upper, lower, o_own = hold((upper, lower, o_own))
     o_half = o_own.shape[0] // 2
     bias, gain, shift = conv_bias[None, :], norm_gain[None, :], norm_bias[None, :]
+    n_grp = lax.axis_size("grp")
+    sign = 1 - 2 * (lax.axis_index("grp") % 2)
     place = jnp.arange(n_dp, dtype=jnp.int32)
     chip = place // 2
-    step = jnp.where(chip == 2, -2, jnp.where(chip == 3, 4, 2 * chip))
-    index = ((me + step) % n_dp) ^ (place % 2)
-
-    next_a, last_b = from_next(upper), from_last(lower)
-    next_b, last_a = from_next(lower), from_last(upper)
+    v_step = jnp.where(chip == 1, 4, jnp.where(chip == 2, 2, jnp.where(chip == 3, -2, 0)) * sign)
+    o_step = jnp.where(chip == 2, -2, jnp.where(chip == 3, 4, 2 * chip))
+    v_index = ((me + v_step) % n_dp) ^ (place % 2)
+    o_index = ((me + o_step) % n_dp) ^ (place % 2)
+
+    def along(step, a):
+        pairs = []
+        for g in range(n_grp):
+            away = step if g % 2 == 0 else -step
+            pairs += [(g * n_dp + i, g * n_dp + (i - away) % n_dp) for i in range(n_dp)]
+        return lax.ppermute(a, ("grp", "dp"), pairs)
+
+    def from_group(a):
+        return lax.ppermute(a, "grp", [(g, g ^ 1) for g in range(n_grp)])
+
+    near_a, near_b = along(2, upper), along(-2, lower)
     rows = jnp.concatenate([halo, tokens], axis=0)
     own_swap = [from_core(upper), from_core(lower)]
-    conv_a = conv_blocks(rows, [[upper, lower], own_swap], index, 0, conv_taps, bias)
-    next_a, last_b, conv_a = hold((next_a, last_b, conv_a))
-    far_a, far_b = from_next(next_a), from_last(last_b)
-    next_b, last_a, o_send = hold((next_b, last_a, o_own))
-    o_next, o_last = from_next(o_send), from_last(o_send)
-    o_swap = from_core(o_send)
-    swaps = [[from_core(next_a), from_core(next_b)], [from_core(last_a), from_core(last_b)]]
+    far_a, far_b = along(2, near_a), along(-2, near_b)
+    pair_a, pair_b = from_group(near_a), from_group(near_b)
+    o_next, o_last = from_next(o_own), from_last(o_own)
+    conv_a = conv_blocks(rows, [[upper, lower], own_swap], v_index, 0, conv_taps, bias)
+    near_a, near_b, far_a, far_b, conv_a, o_own = hold((near_a, near_b, far_a, far_b, conv_a, o_own))
+    near_swap_a, near_swap_b = from_core(near_a), from_core(near_b)
+    o_swap = from_core(o_own)
     conv_b = conv_blocks(
-        rows, [[next_a, next_b], swaps[0], [last_a, last_b], swaps[1]], index, 2, conv_taps, bias
+        rows, [[far_a, far_b], [from_core(far_a), from_core(far_b)]], v_index, 2, conv_taps, bias
     )
-    far_a, far_b, conv_b = hold((far_a, far_b, conv_b))
-    (swished,) = conv_blocks(
-        rows, [[far_a, far_b], [from_core(far_a), from_core(far_b)]], index, 6, conv_taps, bias,
-        conv_a + conv_b, gain, shift,
-    )
-    o_next, o_last, swished = hold((o_next, o_last, swished))
+    o_next, o_last, conv_b = hold((o_next, o_last, conv_b))
     o_far_a, o_far_b = from_next(o_next[:o_half]), from_last(o_last[o_half:])
     o_swaps = from_core(o_next), from_core(o_last)
-    result = out_blocks(
-        swished, [[o_send], [o_swap], [o_next], [o_swaps[0]], [o_last], [o_swaps[1]]], index, 0, n_dp
+    pair_swap_a, pair_swap_b = from_core(pair_a), from_core(pair_b)
+    (swished,) = conv_blocks(
+        rows,
+        [[near_a, pair_b], [near_swap_a, pair_swap_b], [pair_a, near_b], [pair_swap_a, near_swap_b]],
+        v_index, 4, conv_taps, bias, conv_a + conv_b, gain, shift,
     )
-    o_far_a, o_far_b, result = hold((o_far_a, o_far_b, result))
-    result = out_blocks(
-        swished, [[o_far_a, o_far_b], [from_core(o_far_a), from_core(o_far_b)]], index, 6, n_dp, result
-    )
+    o_far_a, o_far_b, swished = hold((o_far_a, o_far_b, swished))
+    o_far_swap = from_core(o_far_a), from_core(o_far_b)
+    result = out_blocks(swished, [[o_own], [o_swap], [o_next], [o_swaps[0]], [o_last], [o_swaps[1]]], o_index, 0, n_dp)
+    result = out_blocks(swished, [[o_far_a, o_far_b], list(o_far_swap)], o_index, 6, n_dp, result)
     return result[None]
 
 

time: 140 us -> 127 us (0.907)
  waiting for transfers between devices: 32.9 us -> 5.29 us
  starting transfers between devices: 29.1 us -> 42.9 us
    ppermute x13, starting transfers between devices: 15.5 us -> 30 us  [from_core(): return lax.ppermute(a, 'dp', [(i, i ^ 1) for i in range(n_dp)])]
    ppermute x5 -> x2, waiting for transfers between devices: 16.3 us -> 3.34 us  [from_last(): return lax.ppermute(a, 'dp', [(i, (i + 2) % n_dp) for i in range(n_dp)])]
    ppermute x5 -> x2, waiting for transfers between devices: 11.4 us -> 0.01 us  [from_next(): return lax.ppermute(a, 'dp', [(i, (i - 2) % n_dp) for i in range(n_dp)])]
    ppermute x5 -> x2, starting transfers between devices: 10.8 us -> 2.8 us  [from_next(): return lax.ppermute(a, 'dp', [(i, (i - 2) % n_dp) for i in range(n_dp)])]
    ppermute x0 -> x6, starting transfers between devices: none -> 7.42 us  [the longest x4 5.96 us: along(): return lax.ppermute(a, ('grp', 'dp'), pairs)]
    ppermute x13, waiting for transfers between devices: 2.21 us -> 0.03 us  [from_core(): return lax.ppermute(a, 'dp', [(i, i ^ 1) for i in range(n_dp)])]
  transfers between devices with their start and end apart: 24 -> 24, of which waited for: 12 -> 2; matrix products, arithmetic and copies ran while one was open for 3% -> 2% of each run, Pallas kernels for 12% -> 15%
where the time goes in v2:
time: 127 us; the launch traced here: 126 us
  blocking collectives  52.4 us (41%)
  starting transfers between devices  42.9 us (34%)
  Pallas kernels  20.6 us (16%)
  waiting for transfers between devices  5.29 us (4%)
  other arithmetic  3.75 us (3%)
    all_gather x1, blocking collectives, work(): packed = lax.all_gather(packed, 'sp', axis=0)  52.4 us
    ppermute x13, starting transfers between devices, from_core(): return lax.ppermute(a, 'dp', [(i, i ^ 1) for i in range(n_dp)])  30 us
    pallas_call x3, Pallas kernels, conv_blocks(): pl.pallas_call(functools.partial(conv_kernel, counts, first, n_done), out...  15.4 us
    ppermute x4, starting transfers between devices, along(): return lax.ppermute(a, ('grp', 'dp'), pairs)  5.96 us
    pallas_call x2, Pallas kernels, out_blocks(): pl.pallas_call(functools.partial(out_kernel, counts, first), out_shape=ja...  5.27 us
    ppermute x2, waiting for transfers between devices, from_last(): return lax.ppermute(a, 'dp', [(i, (i + 2) % n_dp) for i in range(n_dp)])  3.34 us
    ppermute x2, starting transfers between devices, from_next(): return lax.ppermute(a, 'dp', [(i, (i - 2) % n_dp) for i in range(n_dp)])  2.8 us
  transfers between devices with their start and end apart: 24, of which 2 were waited for; matrix products, arithmetic and copies ran while one was open for 2% of the time, Pallas kernels for 15%

profile of v2, /device:TPU:33, one launch (start us, length us, event | category | flops | bytes accessed | tf_op | source)
XLA Modules:
  0.0 126.5 jit_solution(9638290237430326496)
XLA Ops:
  0.0 0.8 maximum_bitcast_fusion
  0.8 0.8 multiply_convert_fusion.1
  1.6 52.4 %all-gather.1 = f16[16,192,256]{2,1,0:T(8,128)(2,1)S(1)} all-gather(f16[1,192,256]{2,1,0:T(8,128)(2,1)S(1)} %multiply_convert_fusion.1), channel_id=1, replica_groups=mesh['grp'=2,'sp'=16,'dp'=8] {'sp'}, dimensions={0}, use_global_device_ids=true | all-gather | bytes 1671168 | tf_op jit(solution)/shard_map/all_gather | solution.py:213
  53.9 0.4 multiply_convert_fusion
  54.3 0.1 fusion.7
  54.5 3.0 %collective-permute-start.3 = (bf16[1024,256]{1,0:T(8,128)(2,1)S(1)}, bf16[1024,256]{1,0:T(8,128)(2,1)S(1)}, u32[]{:S(2)}, u32[]{:S(2)}) collective-permute-start(bf16[1024,256]{1,0:T(8,128)(2,1)S(1)} %bitcast.20), channel_id=1, source_target_pairs={{0,6},{1,7},{2,0},{3,1},{4,2},{5,3},{6,4},{7,5},{128,130},{129,131... | collective-permute-start | bytes 1572872 | tf_op jit(solution)/shard_map/ppermute | solution.py:236
  57.5 0.0 collective-permute-start.4
  57.5 7.5 %collective-permute-start.7 = (bf16[1024,256]{1,0:T(8,128)(2,1)S(1)}, bf16[1024,256]{1,0:T(8,128)(2,1)}, u32[]{:S(2)}, u32[]{:S(2)}) collective-permute-start(bf16[1024,256]{1,0:T(8,128)(2,1)S(1)} %bitcast.21), channel_id=1, source_target_pairs={{0,1},{1,0},{2,3},{3,2},{4,5},{5,4},{6,7},{7,6},{8,9},{9,8},{10,11... | collective-permute-start | bytes 1572872 | tf_op jit(solution)/shard_map/ppermute | solution.py:205
  65.0 0.0 collective-permute-start.8
  65.0 0.0 collective-permute-done.3.refs_3_
  65.0 3.0 %collective-permute-start.5 = (bf16[1024,256]{1,0:T(8,128)(2,1)S(1)}, bf16[1024,256]{1,0:T(8,128)(2,1)S(1)}, u32[]{:S(2)}, u32[]{:S(2)}) collective-permute-start(bf16[1024,256]{1,0:T(8,128)(2,1)S(1)} %collective-permute-done.3.refs_3_), channel_id=1, source_target_pairs={{0,6},{1,7},{2,0},{3,1},{4,2},{5,3},{6,4},{7,5},{128,130},{129,131... | collective-permute-start | bytes 1572872 | tf_op jit(solution)/shard_map/ppermute | solution.py:236
  67.9 0.0 collective-permute-done.4.refs_8_
  68.0 0.0 collective-permute-start.6
  68.0 0.9 slice_bitcast_fusion
  68.9 1.3 %collective-permute-start.2 = (bf16[32,2048]{1,0:T(8,128)(2,1)S(1)}, bf16[32,2048]{1,0:T(8,128)(2,1)S(1)}, u32[]{:S(2)}, u32[]{:S(2)}) collective-permute-start(bf16[32,2048]{1,0:T(8,128)(2,1)S(1)} %slice_bitcast_fusion), channel_id=1, source_target_pairs={{0,8},{8,16},{16,24},{24,32},{32,40},{40,48},{48,56},{56,64},{64,7... | collective-permute-start | bytes 393224 | tf_op jit(solution)/shard_map/ppermute | solution.py:207
  70.2 1.9 %collective-permute-done.2 = bf16[32,2048]{1,0:T(8,128)(2,1)S(1)} collective-permute-done((bf16[32,2048]{1,0:T(8,128)(2,1)S(1)}, bf16[32,2048]{1,0:T(8,128)(2,1)S(1)}, u32[]{:S(2)}, u32[]{:S(2)}) %collective-permute-start.2) | collective-permute-done | bytes 131104 | tf_op jit(solution)/shard_map/ppermute | solution.py:207
  72.1 2.7 %collective-permute-start = (bf16[1024,256]{1,0:T(8,128)(2,1)S(1)}, bf16[1024,256]{1,0:T(8,128)(2,1)S(1)}, u32[]{:S(2)}, u32[]{:S(2)}) collective-permute-start(bf16[1024,256]{1,0:T(8,128)(2,1)S(1)} %bitcast.13), channel_id=1, source_target_pairs={{0,6},{1,7},{2,0},{3,1},{4,2},{5,3},{6,4},{7,5},{8,14},{9,15},{10,... | collective-permute-start | bytes 1572872 | tf_op jit(solution)/shard_map/ppermute | solution.py:199
  74.8 0.0 collective-permute-done.7.refs_3_
  74.8 0.0 collective-permute-start.13
  74.8 0.0 collective-permute-done.8.refs_4_
  74.8 1.5 %collective-permute-start.16 = (bf16[1024,256]{1,0:T(8,128)(2,1)S(1)}, bf16[1024,256]{1,0:T(8,128)(2,1)S(1)}, u32[]{:S(2)}, u32[]{:S(2)}) collective-permute-start(bf16[1024,256]{1,0:T(8,128)(2,1)S(1)} %collective-permute-done.3.refs_3_), channel_id=1, source_target_pairs={{0,128},{128,0},{1,129},{129,1},{2,130},{130,2},{3,131},{131,3},{4... | collective-permute-start | bytes 1572872 | tf_op jit(solution)/shard_map/ppermute | solution.py:239
  76.3 1.8 %pad_maximum_fusion.refs_0_.refs_2_ = bf16[544,2048]{1,0:T(8,128)(2,1)S(1)} fusion(bf16[512,2048]{1,0:T(8,128)(2,1)} %bitcast.28, bf16[32,2048]{1,0:T(8,128)(2,1)S(1)} %collective-permute-done.2), kind=kLoop, calls=%fused_computation.1 | loop fusion | flops 4456448 | bytes 4456448 | tf_op jit(solution)/shard_map/concatenate | solution.py:242
  78.0 0.0 copy-done
  78.1 3.9 %conv_blocks.2 = (f32[512,128]{1,0:T(8,128)S(1)}, f32[512,128]{1,0:T(8,128)S(1)}) custom-call(s32[8]{0:T(128)S(1)} %fusion.1.index_ref, f32[31,1024]{1,0:T(8,128)S(1)} %copy-done, f32[1,1024]{1,0:T(1,128)S(1)} %bitcast.23, bf16[544,2048]{1,0:T(8,128)(2,1)S(1)} %pad_maximum_fusion.refs_0_.refs_2_, bf16[1024,256]{1,0:T(8,128)(2,1)S(1)} %bitcast.22, ...), custom_call_target="tpu_custom_call" | custom-call | flops 1140850688 | bytes 2228224 | tf_op jit(solution)/shard_map/conv_blocks/pallas_call | solution.py:131
  81.9 0.0 collective-permute-done.5.refs_1_
  81.9 0.0 collective-permute-done.6.refs_2_
  82.0 0.0 copy-start.2
  82.0 0.0 copy-start.3
  82.0 12.3 %collective-permute-start.10 = (bf16[1024,256]{1,0:T(8,128)(2,1)}, bf16[1024,256]{1,0:T(8,128)(2,1)S(1)}, u32[]{:S(2)}, u32[]{:S(2)}) collective-permute-start(bf16[1024,256]{1,0:T(8,128)(2,1)} %collective-permute-done.6.refs_2_), channel_id=1, source_target_pairs={{0,1},{1,0},{2,3},{3,2},{4,5},{5,4},{6,7},{7,6},{8,9},{9,8},{10,11... | collective-permute-start | bytes 1572872 | tf_op jit(solution)/shard_map/ppermute | solution.py:205
  94.3 0.1 collective-permute-start.9
  94.5 0.0 collective-permute-done.refs_2_
  94.5 0.0 collective-permute-start.1
  94.5 0.0 collective-permute-done.13.refs_4_
  94.5 1.1 collective-permute-start.14
  95.6 0.0 collective-permute-done.16.refs_7_
  95.6 5.6 %collective-permute-start.18 = (bf16[1024,256]{1,0:T(8,128)(2,1)S(1)}, bf16[1024,256]{1,0:T(8,128)(2,1)S(1)}, u32[]{:S(2)}, u32[]{:S(2)}) collective-permute-start(bf16[1024,256]{1,0:T(8,128)(2,1)S(1)} %collective-permute-done.4.refs_8_), channel_id=1, source_target_pairs={{0,1},{1,0},{2,3},{3,2},{4,5},{5,4},{6,7},{7,6},{8,9},{9,8},{10,11... | collective-permute-start | bytes 1572872 | tf_op jit(solution)/shard_map/ppermute | solution.py:205
  101.3 0.0 collective-permute-done.10.refs_4_
  101.3 0.0 collective-permute-start.15
  101.3 0.0 collective-permute-done.9.refs_3_
  101.3 0.5 collective-permute-start.17
  101.8 3.7 %conv_blocks.3 = (f32[512,128]{1,0:T(8,128)S(1)}, f32[512,128]{1,0:T(8,128)S(1)}) custom-call(s32[8]{0:T(128)S(1)} %fusion.1.index_ref, f32[31,1024]{1,0:T(8,128)S(1)} %copy-done, f32[1,1024]{1,0:T(1,128)S(1)} %bitcast.24, bf16[544,2048]{1,0:T(8,128)(2,1)S(1)} %pad_maximum_fusion.refs_0_.refs_2_, bf16[1024,256]{1,0:T(8,128)(2,1)S(1)} %collective-permute-done.5.refs_1_, ...), custom_call_target="tpu_custom_call" | custom-call | flops 1140850688 | bytes 2228224 | tf_op jit(solution)/shard_map/conv_blocks/pallas_call | solution.py:131
  105.5 3.3 %collective-permute-done.1.refs_4_ = bf16[1024,256]{1,0:T(8,128)(2,1)S(1)} collective-permute-done((bf16[1024,256]{1,0:T(8,128)(2,1)S(1)}, bf16[1024,256]{1,0:T(8,128)(2,1)S(1)}, u32[]{:S(2)}, u32[]{:S(2)}) %collective-permute-start.1) | collective-permute-done | bytes 524320 | tf_op jit(solution)/shard_map/ppermute | solution.py:202
  108.8 1.2 collective-permute-start.21
  110.0 0.0 collective-permute-done.14.refs_5_
  110.0 0.0 collective-permute-start.22
  110.0 0.0 collective-permute-done.18.refs_10_
  110.0 0.5 collective-permute-start.23
  110.6 0.0 collective-permute-done.15.refs_6_
  110.6 0.1 collective-permute-start.11
  110.8 0.0 collective-permute-done.17.refs_9_
  110.8 1.4 %collective-permute-start.12 = (bf16[512,256]{1,0:T(8,128)(2,1)S(1)}, bf16[512,256]{1,0:T(8,128)(2,1)S(1)}, u32[]{:S(2)}, u32[]{:S(2)}) collective-permute-start(bf16[512,256]{1,0:T(8,128)(2,1)S(1)} %slice.27), channel_id=1, source_target_pairs={{0,2},{1,3},{2,4},{3,5},{4,6},{5,7},{6,0},{7,1},{8,10},{9,11},{10,... | collective-permute-start | bytes 786440 | tf_op jit(solution)/shard_map/ppermute | solution.py:202
  112.2 0.0 copy-done.3
  112.2 7.8 %conv_norm.1.rows_ref = bf16[512,1024]{1,0:T(8,128)(2,1)S(1)} custom-call(s32[8]{0:T(128)S(1)} %fusion.1.index_ref, f32[31,1024]{1,0:T(8,128)S(1)} %copy-done, f32[1,1024]{1,0:T(1,128)S(1)} %bitcast.25, f32[1,1024]{1,0:T(1,128)S(1)} %bitcast.26, f32[1,1024]{1,0:T(1,128)S(1)} %bitcast.27, bf16[544,2048]{1,0:T(8,128)(2,1)S(1)} %pad_maximum_fusion.refs_0_.refs_2_, ...), custom_call_target="tpu_custom_call" | custom-call | flops 2281701376 | bytes 2228224 | tf_op jit(solution)/shard_map/conv_norm/pallas_call | solution.py:131
  120.0 0.0 collective-permute-done.11.refs_0_
  120.0 0.0 collective-permute-done.12.refs_1_
  120.0 0.8 collective-permute-start.19
  120.8 0.1 collective-permute-start.20
  121.0 0.0 collective-permute-done.21.refs_1_
  121.0 0.0 collective-permute-done.22.refs_3_
  121.0 0.0 collective-permute-done.23.refs_5_
  121.0 3.2 %out_blocks.2.refs_4_ = bf16[512,2048]{1,0:T(8,128)(2,1)} custom-call(s32[8]{0:T(128)S(1)} %fusion.index_ref, bf16[512,1024]{1,0:T(8,128)(2,1)S(1)} %conv_norm.1.rows_ref, bf16[1024,256]{1,0:T(8,128)(2,1)S(1)} %bitcast.16, bf16[1024,256]{1,0:T(8,128)(2,1)S(1)} %collective-permute-done.21.refs_1_, bf16[1024,256]{1,0:T(8,128)(2,1)S(1)} %collective-permute-done.refs_2_, ...), custom_call_target="tpu_custom_call" | custom-call | flops 1610612736 | bytes 3145728 | tf_op jit(solution)/shard_map/out_blocks/pallas_call | solution.py:177
  124.2 0.0 collective-permute-done.19.refs_2_
  124.2 0.0 collective-permute-done.20.refs_3_
  124.2 2.1 %out_blocks.3 = bf16[512,2048]{1,0:T(8,128)(2,1)} custom-call(s32[8]{0:T(128)S(1)} %fusion.index_ref, bf16[512,1024]{1,0:T(8,128)(2,1)S(1)} %conv_norm.1.rows_ref, bf16[512,256]{1,0:T(8,128)(2,1)S(1)} %collective-permute-done.11.refs_0_, bf16[512,256]{1,0:T(8,128)(2,1)S(1)} %collective-permute-done.12.refs_1_, ...), custom_call_target="tpu_custom_call", output_to_operand_aliasing={{}: (6, {})} | custom-call | flops 536870912 | bytes 3145728 | tf_op jit(solution)/shard_map/out_blocks/pallas_call | solution.py:177
  (9 shorter events, 0.1 us)
Async XLA Ops:
  54.5 10.5 %collective-permute-start.3 = (bf16[1024,256]{1,0:T(8,128)(2,1)S(1)}, bf16[1024,256]{1,0:T(8,128)(2,1)S(1)}, u32[]{:S(2)}, u32[]{:S(2)}) collective-permute-start(bf16[1024,256]{1,0:T(8,128)(2,1)S(1)} %bitcast.20), channel_id=1, source_target_pairs={{0,6},{1,7},{2,0},{3,1},{4,2},{5,3},{6,4},{7,5},{128,130},{129,131... | collective-permute-start | bytes 1572872 | tf_op jit(solution)/shard_map/ppermute | solution.py:236
  57.5 10.5 %collective-permute-start.4 = (bf16[1024,256]{1,0:T(8,128)(2,1)S(1)}, bf16[1024,256]{1,0:T(8,128)(2,1)S(1)}, u32[]{:S(2)}, u32[]{:S(2)}) collective-permute-start(bf16[1024,256]{1,0:T(8,128)(2,1)S(1)} %bitcast.17), channel_id=1, source_target_pairs={{0,2},{1,3},{2,4},{3,5},{4,6},{5,7},{6,0},{7,1},{128,134},{129,135... | collective-permute-start | bytes 1572872 | tf_op jit(solution)/shard_map/ppermute | solution.py:236
  57.5 17.3 %collective-permute-start.7 = (bf16[1024,256]{1,0:T(8,128)(2,1)S(1)}, bf16[1024,256]{1,0:T(8,128)(2,1)}, u32[]{:S(2)}, u32[]{:S(2)}) collective-permute-start(bf16[1024,256]{1,0:T(8,128)(2,1)S(1)} %bitcast.21), channel_id=1, source_target_pairs={{0,1},{1,0},{2,3},{3,2},{4,5},{5,4},{6,7},{7,6},{8,9},{9,8},{10,11... | collective-permute-start | bytes 1572872 | tf_op jit(solution)/shard_map/ppermute | solution.py:205
  65.0 9.8 %collective-permute-start.8 = (bf16[1024,256]{1,0:T(8,128)(2,1)S(1)}, bf16[1024,256]{1,0:T(8,128)(2,1)}, u32[]{:S(2)}, u32[]{:S(2)}) collective-permute-start(bf16[1024,256]{1,0:T(8,128)(2,1)S(1)} %bitcast.18), channel_id=1, source_target_pairs={{0,1},{1,0},{2,3},{3,2},{4,5},{5,4},{6,7},{7,6},{8,9},{9,8},{10,11... | collective-permute-start | bytes 1572872 | tf_op jit(solution)/shard_map/ppermute | solution.py:205
  65.0 16.9 %collective-permute-start.5 = (bf16[1024,256]{1,0:T(8,128)(2,1)S(1)}, bf16[1024,256]{1,0:T(8,128)(2,1)S(1)}, u32[]{:S(2)}, u32[]{:S(2)}) collective-permute-start(bf16[1024,256]{1,0:T(8,128)(2,1)S(1)} %collective-permute-done.3.refs_3_), channel_id=1, source_target_pairs={{0,6},{1,7},{2,0},{3,1},{4,2},{5,3},{6,4},{7,5},{128,130},{129,131... | collective-permute-start | bytes 1572872 | tf_op jit(solution)/shard_map/ppermute | solution.py:236
  68.0 14.0 %collective-permute-start.6 = (bf16[1024,256]{1,0:T(8,128)(2,1)S(1)}, bf16[1024,256]{1,0:T(8,128)(2,1)}, u32[]{:S(2)}, u32[]{:S(2)}) collective-permute-start(bf16[1024,256]{1,0:T(8,128)(2,1)S(1)} %collective-permute-done.4.refs_8_), channel_id=1, source_target_pairs={{0,2},{1,3},{2,4},{3,5},{4,6},{5,7},{6,0},{7,1},{128,134},{129,135... | collective-permute-start | bytes 1572872 | tf_op jit(solution)/shard_map/ppermute | solution.py:236
  68.9 3.2 %collective-permute-start.2 = (bf16[32,2048]{1,0:T(8,128)(2,1)S(1)}, bf16[32,2048]{1,0:T(8,128)(2,1)S(1)}, u32[]{:S(2)}, u32[]{:S(2)}) collective-permute-start(bf16[32,2048]{1,0:T(8,128)(2,1)S(1)} %slice_bitcast_fusion), channel_id=1, source_target_pairs={{0,8},{8,16},{16,24},{24,32},{32,40},{40,48},{48,56},{56,64},{64,7... | collective-permute-start | bytes 393224 | tf_op jit(solution)/shard_map/ppermute | solution.py:207
  72.1 22.4 %collective-permute-start = (bf16[1024,256]{1,0:T(8,128)(2,1)S(1)}, bf16[1024,256]{1,0:T(8,128)(2,1)S(1)}, u32[]{:S(2)}, u32[]{:S(2)}) collective-permute-start(bf16[1024,256]{1,0:T(8,128)(2,1)S(1)} %bitcast.13), channel_id=1, source_target_pairs={{0,6},{1,7},{2,0},{3,1},{4,2},{5,3},{6,4},{7,5},{8,14},{9,15},{10,... | collective-permute-start | bytes 1572872 | tf_op jit(solution)/shard_map/ppermute | solution.py:199
  74.8 19.7 %collective-permute-start.13 = (bf16[1024,256]{1,0:T(8,128)(2,1)S(1)}, bf16[1024,256]{1,0:T(8,128)(2,1)S(1)}, u32[]{:S(2)}, u32[]{:S(2)}) collective-permute-start(bf16[1024,256]{1,0:T(8,128)(2,1)S(1)} %collective-permute-done.4.refs_8_), channel_id=1, source_target_pairs={{0,128},{128,0},{1,129},{129,1},{2,130},{130,2},{3,131},{131,3},{4... | collective-permute-start | bytes 1572872 | tf_op jit(solution)/shard_map/ppermute | solution.py:239
  74.8 20.8 %collective-permute-start.16 = (bf16[1024,256]{1,0:T(8,128)(2,1)S(1)}, bf16[1024,256]{1,0:T(8,128)(2,1)S(1)}, u32[]{:S(2)}, u32[]{:S(2)}) collective-permute-start(bf16[1024,256]{1,0:T(8,128)(2,1)S(1)} %collective-permute-done.3.refs_3_), channel_id=1, source_target_pairs={{0,128},{128,0},{1,129},{129,1},{2,130},{130,2},{3,131},{131,3},{4... | collective-permute-start | bytes 1572872 | tf_op jit(solution)/shard_map/ppermute | solution.py:239
  76.3 1.8 %copy-start = (f32[31,1024]{1,0:T(8,128)S(1)}, f32[31,1024]{1,0:T(8,128)}, u32[]{:S(2)}) copy-start(f32[31,1024]{1,0:T(8,128)} %taps_ref.5) | copy-start | bytes 380932
  76.3 1.8 %copy-start.1 = (f32[1024]{0:T(1024)S(1)}, f32[1024]{0:T(1024)}, u32[]{:S(2)}) copy-start(f32[1024]{0:T(1024)} %param.12) | copy-start | bytes 12292
  82.0 30.2 %copy-start.2 = (f32[1024]{0:T(1024)S(1)}, f32[1024]{0:T(1024)}, u32[]{:S(2)}) copy-start(f32[1024]{0:T(1024)} %param.13) | copy-start | bytes 12292
  82.0 30.2 %copy-start.3 = (f32[1024]{0:T(1024)S(1)}, f32[1024]{0:T(1024)}, u32[]{:S(2)}) copy-start(f32[1024]{0:T(1024)} %param.14) | copy-start | bytes 12292
  82.0 19.3 %collective-permute-start.10 = (bf16[1024,256]{1,0:T(8,128)(2,1)}, bf16[1024,256]{1,0:T(8,128)(2,1)S(1)}, u32[]{:S(2)}, u32[]{:S(2)}) collective-permute-start(bf16[1024,256]{1,0:T(8,128)(2,1)} %collective-permute-done.6.refs_2_), channel_id=1, source_target_pairs={{0,1},{1,0},{2,3},{3,2},{4,5},{5,4},{6,7},{7,6},{8,9},{9,8},{10,11... | collective-permute-start | bytes 1572872 | tf_op jit(solution)/shard_map/ppermute | solution.py:205
  94.3 6.9 %collective-permute-start.9 = (bf16[1024,256]{1,0:T(8,128)(2,1)S(1)}, bf16[1024,256]{1,0:T(8,128)(2,1)S(1)}, u32[]{:S(2)}, u32[]{:S(2)}) collective-permute-start(bf16[1024,256]{1,0:T(8,128)(2,1)S(1)} %collective-permute-done.5.refs_1_), channel_id=1, source_target_pairs={{0,1},{1,0},{2,3},{3,2},{4,5},{5,4},{6,7},{7,6},{8,9},{9,8},{10,11... | collective-permute-start | bytes 1572872 | tf_op jit(solution)/shard_map/ppermute | solution.py:205
  94.5 14.3 %collective-permute-start.1 = (bf16[1024,256]{1,0:T(8,128)(2,1)S(1)}, bf16[1024,256]{1,0:T(8,128)(2,1)S(1)}, u32[]{:S(2)}, u32[]{:S(2)}) collective-permute-start(bf16[1024,256]{1,0:T(8,128)(2,1)S(1)} %bitcast.14), channel_id=1, source_target_pairs={{0,2},{1,3},{2,4},{3,5},{4,6},{5,7},{6,0},{7,1},{8,10},{9,11},{10,... | collective-permute-start | bytes 1572872 | tf_op jit(solution)/shard_map/ppermute | solution.py:202
  94.5 15.5 %collective-permute-start.14 = (bf16[1024,256]{1,0:T(8,128)(2,1)S(1)}, bf16[1024,256]{1,0:T(8,128)(2,1)S(1)}, u32[]{:S(2)}, u32[]{:S(2)}) collective-permute-start(bf16[1024,256]{1,0:T(8,128)(2,1)S(1)} %collective-permute-done.3.refs_3_), channel_id=1, source_target_pairs={{0,1},{1,0},{2,3},{3,2},{4,5},{5,4},{6,7},{7,6},{8,9},{9,8},{10,11... | collective-permute-start | bytes 1572872 | tf_op jit(solution)/shard_map/ppermute | solution.py:205
  95.6 14.4 %collective-permute-start.18 = (bf16[1024,256]{1,0:T(8,128)(2,1)S(1)}, bf16[1024,256]{1,0:T(8,128)(2,1)S(1)}, u32[]{:S(2)}, u32[]{:S(2)}) collective-permute-start(bf16[1024,256]{1,0:T(8,128)(2,1)S(1)} %collective-permute-done.4.refs_8_), channel_id=1, source_target_pairs={{0,1},{1,0},{2,3},{3,2},{4,5},{5,4},{6,7},{7,6},{8,9},{9,8},{10,11... | collective-permute-start | bytes 1572872 | tf_op jit(solution)/shard_map/ppermute | solution.py:205
  101.3 9.3 %collective-permute-start.15 = (bf16[1024,256]{1,0:T(8,128)(2,1)S(1)}, bf16[1024,256]{1,0:T(8,128)(2,1)S(1)}, u32[]{:S(2)}, u32[]{:S(2)}) collective-permute-start(bf16[1024,256]{1,0:T(8,128)(2,1)S(1)} %collective-permute-done.13.refs_4_), channel_id=1, source_target_pairs={{0,1},{1,0},{2,3},{3,2},{4,5},{5,4},{6,7},{7,6},{8,9},{9,8},{10,11... | collective-permute-start | bytes 1572872 | tf_op jit(solution)/shard_map/ppermute | solution.py:205
  101.3 9.5 %collective-permute-start.17 = (bf16[1024,256]{1,0:T(8,128)(2,1)S(1)}, bf16[1024,256]{1,0:T(8,128)(2,1)S(1)}, u32[]{:S(2)}, u32[]{:S(2)}) collective-permute-start(bf16[1024,256]{1,0:T(8,128)(2,1)S(1)} %collective-permute-done.16.refs_7_), channel_id=1, source_target_pairs={{0,1},{1,0},{2,3},{3,2},{4,5},{5,4},{6,7},{7,6},{8,9},{9,8},{10,11... | collective-permute-start | bytes 1572872 | tf_op jit(solution)/shard_map/ppermute | solution.py:205
  108.8 12.2 %collective-permute-start.21 = (bf16[1024,256]{1,0:T(8,128)(2,1)S(1)}, bf16[1024,256]{1,0:T(8,128)(2,1)S(1)}, u32[]{:S(2)}, u32[]{:S(2)}) collective-permute-start(bf16[1024,256]{1,0:T(8,128)(2,1)S(1)} %bitcast.15), channel_id=1, source_target_pairs={{0,1},{1,0},{2,3},{3,2},{4,5},{5,4},{6,7},{7,6},{8,9},{9,8},{10,11... | collective-permute-start | bytes 1572872 | tf_op jit(solution)/shard_map/ppermute | solution.py:205
  110.0 10.9 %collective-permute-start.22 = (bf16[1024,256]{1,0:T(8,128)(2,1)S(1)}, bf16[1024,256]{1,0:T(8,128)(2,1)S(1)}, u32[]{:S(2)}, u32[]{:S(2)}) collective-permute-start(bf16[1024,256]{1,0:T(8,128)(2,1)S(1)} %collective-permute-done.refs_2_), channel_id=1, source_target_pairs={{0,1},{1,0},{2,3},{3,2},{4,5},{5,4},{6,7},{7,6},{8,9},{9,8},{10,11... | collective-permute-start | bytes 1572872 | tf_op jit(solution)/shard_map/ppermute | solution.py:205
  110.0 10.9 %collective-permute-start.23 = (bf16[1024,256]{1,0:T(8,128)(2,1)S(1)}, bf16[1024,256]{1,0:T(8,128)(2,1)S(1)}, u32[]{:S(2)}, u32[]{:S(2)}) collective-permute-start(bf16[1024,256]{1,0:T(8,128)(2,1)S(1)} %collective-permute-done.1.refs_4_), channel_id=1, source_target_pairs={{0,1},{1,0},{2,3},{3,2},{4,5},{5,4},{6,7},{7,6},{8,9},{9,8},{10,11... | collective-permute-start | bytes 1572872 | tf_op jit(solution)/shard_map/ppermute | solution.py:205
  110.6 9.4 %collective-permute-start.11 = (bf16[512,256]{1,0:T(8,128)(2,1)S(1)}, bf16[512,256]{1,0:T(8,128)(2,1)S(1)}, u32[]{:S(2)}, u32[]{:S(2)}) collective-permute-start(bf16[512,256]{1,0:T(8,128)(2,1)S(1)} %slice.26), channel_id=1, source_target_pairs={{0,6},{1,7},{2,0},{3,1},{4,2},{5,3},{6,4},{7,5},{8,14},{9,15},{10,... | collective-permute-start | bytes 786440 | tf_op jit(solution)/shard_map/ppermute | solution.py:199
  110.8 9.3 %collective-permute-start.12 = (bf16[512,256]{1,0:T(8,128)(2,1)S(1)}, bf16[512,256]{1,0:T(8,128)(2,1)S(1)}, u32[]{:S(2)}, u32[]{:S(2)}) collective-permute-start(bf16[512,256]{1,0:T(8,128)(2,1)S(1)} %slice.27), channel_id=1, source_target_pairs={{0,2},{1,3},{2,4},{3,5},{4,6},{5,7},{6,0},{7,1},{8,10},{9,11},{10,... | collective-permute-start | bytes 786440 | tf_op jit(solution)/shard_map/ppermute | solution.py:202
  120.0 4.2 %collective-permute-start.19 = (bf16[512,256]{1,0:T(8,128)(2,1)S(1)}, bf16[512,256]{1,0:T(8,128)(2,1)S(1)}, u32[]{:S(2)}, u32[]{:S(2)}) collective-permute-start(bf16[512,256]{1,0:T(8,128)(2,1)S(1)} %collective-permute-done.11.refs_0_), channel_id=1, source_target_pairs={{0,1},{1,0},{2,3},{3,2},{4,5},{5,4},{6,7},{7,6},{8,9},{9,8},{10,11... | collective-permute-start | bytes 786440 | tf_op jit(solution)/shard_map/ppermute | solution.py:205
  120.8 3.4 %collective-permute-start.20 = (bf16[512,256]{1,0:T(8,128)(2,1)S(1)}, bf16[512,256]{1,0:T(8,128)(2,1)S(1)}, u32[]{:S(2)}, u32[]{:S(2)}) collective-permute-start(bf16[512,256]{1,0:T(8,128)(2,1)S(1)} %collective-permute-done.12.refs_1_), channel_id=1, source_target_pairs={{0,1},{1,0},{2,3},{3,2},{4,5},{5,4},{6,7},{7,6},{8,9},{9,8},{10,11... | collective-permute-start | bytes 786440 | tf_op jit(solution)/shard_map/ppermute | solution.py:205
